TPU v7x, 32 devices: a whole 2x2x4 slice. The times are simulated.
32 devices in a mesh: fs: 8 (over z, y), tp: 4 (over x, core).
Axes of the slice: x: 2, y: 2, z: 4, core: 2. Of those that a mesh axis runs over, the one named last changes fastest.
Arguments:
- tokens: bfloat16 [4096, 4096], P('fs'), may hold values from -6 to 6
- norm_gain: float32 [4096], P('fs'), may hold values from 0.1 to 1.9
- gate_train: float32 [8, 4096, 1024], P(None, 'fs', 'tp'), may hold values from -0.09375 to 0.09375
- up_train: float32 [8, 4096, 1024], P(None, 'fs', 'tp'), may hold values from -0.09375 to 0.09375
- down_train: float32 [8, 1024, 4096], P(None, 'fs', 'tp'), may hold values from -0.1875 to 0.1875
- shared_gate_train: float32 [4096, 1024], P('fs', 'tp'), may hold values from -0.09375 to 0.09375
- shared_up_train: float32 [4096, 1024], P('fs', 'tp'), may hold values from -0.09375 to 0.09375
- shared_down_train: float32 [1024, 4096], P('fs', 'tp'), may hold values from -0.1875 to 0.1875
- route_expert: int32 [4096, 2], P('fs'), may hold values from 0 to 7, all different within a row; in each aligned block of 512 rows (0 to 511, 512 to 1023, ...) at most 192 rows name the same one
- route_weight: float32 [4096, 2], P('fs'), may hold values from 0.1 to 1
Outputs:
- expert_gate: bfloat16 [8, 4096, 1024], P('fs', None, 'tp')
- expert_up: bfloat16 [8, 4096, 1024], P('fs', None, 'tp')
- expert_down: bfloat16 [8, 1024, 4096], P('fs', 'tp')
- shared_gate: bfloat16 [4096, 1024], P(None, 'tp')
- shared_up: bfloat16 [4096, 1024], P(None, 'tp')
- shared_down: bfloat16 [1024, 4096], P('tp')
- mixed: bfloat16 [4096, 4096], P('fs', 'tp')
Inputs may be any that keep to these rules, and one draw needn't show every extreme that they name: `route_expert`: each row names 2 different experts. Within each aligned block of 512 rows no expert is named by more than 192 rows, a bound that some block reaches in every draw.
All inputs are finite; a program needn't handle non-finite values.
Results may differ from a plain program's by a relative error of at most 0.015.
Values may be sent and summed in bfloat16 or wider, within the bound.
A program may use at most 128 MiB of HBM per device.

v0:
```python
import functools

import jax
import jax.numpy as jnp
from jax import lax
from jax.experimental import pallas as pl
from jax.experimental.pallas import tpu as pltpu
from jax.sharding import PartitionSpec as P

norm_eps = 1e-06
cores = 2
MESH = pl.DeviceIdType.MESH
F32, BF16 = jnp.float32, jnp.bfloat16


class Sizes:
    def __init__(self, experts, pieces, tokens, gate, down, sgate, sdown, top):
        self.E, self.P = experts, pieces
        self.C = pieces // cores
        long = 1
        while long * long < experts:
            long *= 2
        self.Z, self.Y = long, experts // long
        self.half = experts // 2
        self.T, self.D = tokens
        self.cap = 3 * self.T * top // (2 * experts)
        self.Dr, self.Hc = gate[1:]
        self.Hr, self.Dc = down[1:]
        self.Dr2, self.Sc = sgate
        self.Sr = sdown[0]
        self.per = experts // pieces
        self.g = 1
        while self.g * self.cap % 128:
            self.g *= 2
        self.groups = experts // self.g
        self.M = self.g * self.cap
        self.nt = min(256, self.Dc)


def kernel(
    S,
    tokens, gate_t, up_t, down_t, sgate_t, sup_t, sdown_t, gain, rows_of, cols_of,
    eg, eu, ed, sg, su, sd, mixed,
    nrm, tok, info, shb, sdb, gst, gub, dst, dnb, rows, yst, hid, res, ret, acc, shid, outb,
    wbuf, dbuf,
    ld_sem, tk_ld, out_sem,
    tok_s, tok_r, info_s, info_r, sh_s, sh_r, shy_s, sd_s, sd_r, sdy_s,
    gu_s, gu_r, dn_s, dn_r, y_s, rows_r, x_s, part_s, part_r,
    hid_s, hid_r, shid_s, shid_r, edo_s, edo_r, sdo_s, sdo_r, ret_s, ret_r,
):
    E, Pn, C, Z, Y, half, per = S.E, S.P, S.C, S.Z, S.Y, S.half, S.per
    cap, Dc, Hc, Sc, nt = S.cap, S.Dc, S.Hc, S.Sc, S.nt
    f, t = lax.axis_index("fs"), lax.axis_index("tp")
    z, y = f // Y, f % Y
    x, c = t // cores, t % cores
    h, fo = f // half, f % half

    def ring(k, count, at, back=False):
        mid = count // 2
        far = k // mid
        off = k % mid + far
        side = (at // mid + 1 + far) % 2
        step = at % mid - off + count if back else at % mid + off
        return side * mid + step % mid

    def peer(k):
        return ring(k, E, f)

    def source(k):
        return ring(k, E, f, True)

    def rcopy(src, dst, ssem, rsem, to):
        return pltpu.make_async_remote_copy(
            src_ref=src, dst_ref=dst, send_sem=ssem, recv_sem=rsem,
            device_id=to, device_id_type=MESH,
        )

    def arrived(ref, rsem):
        rcopy(ref, ref, out_sem.at[0], rsem, ((f + 1) % E, t)).wait_recv()

    def sent(ref, ssem):
        rcopy(ref, ref, ssem, out_sem.at[0], ((f + 1) % E, t)).wait_send()

    def loop(count, body, start=0):
        lax.fori_loop(start, count, lambda i, v: (body(i), v)[1], 0)

    def load_w(k, slot):
        e = peer(k)
        return [
            pltpu.make_async_copy(w.at[e], wbuf.at[slot, i], ld_sem.at[slot, i])
            for i, w in ((0, gate_t), (1, up_t))
        ]

    def load_d(k, slot):
        return pltpu.make_async_copy(down_t.at[peer(k)], dbuf.at[slot], ld_sem.at[slot, 2])

    tok_load = pltpu.make_async_copy(tokens, nrm, tk_ld.at[0])
    tok_load.start()
    sh_loads = [
        pltpu.make_async_copy(sgate_t, wbuf.at[1, 0], ld_sem.at[1, 0]),
        pltpu.make_async_copy(sup_t, wbuf.at[1, 1], ld_sem.at[1, 1]),
        pltpu.make_async_copy(sdown_t, dbuf.at[1], ld_sem.at[1, 2]),
    ]
    for copy in sh_loads + load_w(0, 0) + [load_d(0, 0)]:
        copy.start()

    T = S.T
    wide = max(16, E)
    r0, r1 = rows_of[0:1, :], rows_of[1:2, :]
    names = lax.broadcasted_iota(jnp.int32, (wide, T), 0).astype(F32)
    hit0, hit1 = r0 == names, r1 == names
    chosen = (hit0 | hit1).astype(F32).astype(BF16)
    before = lax.broadcasted_iota(jnp.int32, (T, T), 0) < lax.broadcasted_iota(
        jnp.int32, (T, T), 1
    )
    count = jnp.dot(chosen, before.astype(F32).astype(BF16), preferred_element_type=F32)
    s0 = jnp.sum(jnp.where(hit0, count, 0.0), axis=0, keepdims=True)
    s1 = jnp.sum(jnp.where(hit1, count, 0.0), axis=0, keepdims=True)
    info[z, 0:1, :] = r0
    info[z, 1:2, :] = r1
    info[z, 2:3, :] = s0
    info[z, 3:4, :] = s1

    tok_load.wait()
    tile = min(64, T)

    def normalise(i):
        at = pl.ds(pl.multiple_of(i * tile, tile), tile)
        v = nrm[at, :].astype(F32)
        v = v * lax.rsqrt(jnp.mean(v * v, axis=1, keepdims=True) + norm_eps)
        nrm[at, :] = v.astype(BF16)
        tok[z, at, :] = nrm[at, pl.ds(pl.multiple_of(t * Dc, Dc), Dc)]

    loop(T // tile, normalise)

    for copy in sh_loads:
        copy.wait()
    shb[f, :, 0:Sc] = (gain[...] * wbuf[1, 0]).astype(BF16)
    shb[f, :, Sc:] = (gain[...] * wbuf[1, 1]).astype(BF16)
    sdb[f] = dbuf[1].astype(BF16)

    def line(buf, slot_of, ssem, rsem, hop):
        for d, ok_next in ((0, z + 1 < Z), (1, z > 0)):
            zs = z - hop if d == 0 else z + hop
            there = (zs >= 0) if d == 0 else (zs < Z)
            slot = slot_of(jnp.clip(zs, 0, Z - 1))
            nxt = (f + Y if d == 0 else f - Y, t)

            @pl.when(there)
            def _():
                if hop:
                    arrived(buf.at[slot], rsem.at[slot])

                @pl.when(ok_next)
                def _():
                    rcopy(
                        buf.at[slot], buf.at[slot], ssem.at[d, hop], rsem.at[slot], nxt
                    ).start()

    def line_drain(buf, slot_of, ssem):
        for hop in range(Z - 1):
            for d, ok_next in ((0, z + 1 < Z), (1, z > 0)):
                zs = z - hop if d == 0 else z + hop
                there = (zs >= 0) if d == 0 else (zs < Z)
                slot = slot_of(jnp.clip(zs, 0, Z - 1))

                @pl.when(there & ok_next)
                def _():
                    sent(buf.at[slot], ssem.at[d, hop])

    by_z = lambda zs: zs
    by_f = lambda zs: zs * Y + y

    for i in range(1, Z):
        zo = (z + i) % Z
        rcopy(info.at[z], info.at[z], info_s.at[i - 1], info_r.at[z], (zo * Y + y, t)).start()
    line(tok, by_z, tok_s, tok_r, 0)

    def convert_gu(k):
        slot = k % 2
        for copy in load_w(k, slot):
            copy.wait()

        @pl.when(k + 1 < E)
        def _():
            for copy in load_w(k + 1, 1 - slot):
                copy.start()

        for i in range(2):
            gst[k, :, i * Hc : (i + 1) * Hc] = (gain[...] * wbuf[slot, i]).astype(BF16)

    def convert_dn(k):
        slot = k % 2
        load_d(k, slot).wait()

        @pl.when(k + 1 < E)
        def _():
            load_d(k + 1, 1 - slot).start()

        dst[k] = dbuf[slot].astype(BF16)

    loop(E, convert_gu)

    def shared_y(zs):
        s = by_f(zs)
        for j in range(1, Y):
            to = (z * Y + (y + j) % Y, t)
            rcopy(shb.at[s], shb.at[s], shy_s.at[j - 1], sh_r.at[s], to).start()
            rcopy(sdb.at[s], sdb.at[s], sdy_s.at[j - 1], sd_r.at[s], to).start()

    line(shb, by_f, sh_s, sh_r, 0)
    line(sdb, by_f, sd_s, sd_r, 0)
    shared_y(z)
    loop(E, convert_dn)
    gub[f] = gst[E - 1]
    dnb[f] = dst[E - 1]

    def x_out(s):
        for i in range(1, C):
            to = (f, (x + i) % C * cores + c)
            rcopy(rows.at[t, s], rows.at[t, s], x_s.at[i - 1], rows_r.at[t, s], to).start()
        rcopy(rows.at[t, s], rows.at[t, s], part_s.at[0], part_r.at[0], (f, x * cores + 1 - c)).start()

    def pick(zs):
        s = by_f(zs)
        for j in list(range(1, Y)) + [0]:
            e = (z * Y + (y + j) % Y).astype(F32)
            slots = lax.broadcasted_iota(jnp.int32, (cap, T), 0).astype(F32)
            got = (info[zs, 0:1, :] == e) & (info[zs, 2:3, :] == slots)
            got |= (info[zs, 1:2, :] == e) & (info[zs, 3:4, :] == slots)
            got = got.astype(F32).astype(BF16)

            def part(n):
                at = pl.ds(pl.multiple_of(n * nt, nt), nt)
                block = jnp.dot(got, tok[zs, :, at], preferred_element_type=F32).astype(BF16)
                if j:
                    yst[zs, j - 1, :, at] = block
                else:
                    rows[t, s, :, at] = block

            loop(Dc // nt, part)
        for j in range(1, Y):
            to = (z * Y + (y + j) % Y, t)
            rcopy(
                yst.at[zs, j - 1], rows.at[t, s], y_s.at[j - 1], rows_r.at[t, s], to
            ).start()
        x_out(s)

    pick(z)

    def send_gu(k):
        e = peer(k)
        rcopy(gst.at[k], gub.at[f], gu_s.at[k], gu_r.at[f], (e, t)).start()

    def send_dn(k):
        e = peer(k)
        rcopy(dst.at[k], dnb.at[f], dn_s.at[k], dn_r.at[f], (e, t)).start()

    def arrivals(hop):
        for zs, there in ((z - hop, z - hop >= 0), (z + hop, z + hop < Z)):
            at = jnp.clip(zs, 0, Z - 1)

            @pl.when(there)
            def _():
                shared_y(at)
                arrived(info.at[at], info_r.at[at])
                pick(at)

    for hop in range(1, Z):
        line(tok, by_z, tok_s, tok_r, hop)
        line(shb, by_f, sh_s, sh_r, hop)
        line(sdb, by_f, sd_s, sd_r, hop)
        if hop == 1:
            loop(half, send_gu)
        if hop == Z - 2 or Z <= 2:
            loop(E - 1, send_gu, half)
            loop(E - 1, send_dn)
        arrivals(hop)

    for j in range(1, Y):
        for zs in range(Z):
            s = zs * Y + (y + j) % Y
            arrived(rows.at[t, s], rows_r.at[t, s])
            x_out(s)
    for i in range(1, C):
        to_t = (x + i) % C * cores + c

        def forward(s):
            arrived(rows.at[to_t, s], rows_r.at[to_t, s])
            rcopy(
                rows.at[to_t, s], rows.at[to_t, s], part_s.at[i], part_r.at[i],
                (f, x * cores + 1 - c),
            ).start()

        loop(E, forward)

    for j in range(1, Y):
        for zs in range(Z):
            s = zs * Y + (y + j) % Y
            arrived(shb.at[s], sh_r.at[s])
            arrived(sdb.at[s], sd_r.at[s])

    def put(src, dst_ref, i):
        copy = pltpu.make_async_copy(src, dst_ref, out_sem.at[i])
        copy.start()
        return copy

    puts = [put(shb.at[:, :, pl.ds(0, Sc)], sg, 1), put(shb.at[:, :, pl.ds(Sc, Sc)], su, 2)]
    own_cols = pl.ds(pl.multiple_of(t * Dc, Dc), Dc)

    def spread(buf, out, ssem, rsem, i):
        for k in range(1, Pn):
            tt = (t + k) % Pn
            rcopy(
                buf.at[pl.ds(tt * per, per)], out.at[:, :, own_cols], ssem.at[k - 1],
                rsem.at[t], (f, tt),
            ).start()
        return put(buf.at[pl.ds(t * per, per)], out.at[:, :, own_cols], i)

    def spread_wait(buf, out, ssem, rsem):
        for k in range(1, Pn):
            tt = (t + k) % Pn
            sent(buf.at[pl.ds(tt * per, per)], ssem.at[k - 1])
            at = pl.ds(pl.multiple_of(tt * Dc, Dc), Dc)
            arrived(out.at[:, :, at], rsem.at[tt])

    puts.append(spread(sdb, sd, sdo_s, sdo_r, 3))

    def act(v, width):
        gate, up = v[:, :width], v[:, width:]
        return (gate / (1.0 + jnp.exp(-gate)) * up).astype(BF16)

    mt = min(256, T)

    def shared_in(m):
        at = pl.ds(pl.multiple_of(m * mt, mt), mt)
        total = None
        for q in range(Pn):
            w = shb[q * per : (q + 1) * per].reshape(Dc, 2 * Sc)
            term = jnp.dot(nrm[at, q * Dc : (q + 1) * Dc], w, preferred_element_type=F32)
            total = term if total is None else total + term
        shid[t, at, :] = act(total, Sc)

    loop(T // mt, shared_in)

    def rows_waits():
        part = x * cores + 1 - c
        arrived(rows.at[part], part_r.at[0])
        for i in range(1, C):
            arrived(rows.at[(x + i) % C * cores + 1 - c], part_r.at[i])

    rows_waits()
    for k in range(1, Pn):
        rcopy(shid.at[t], shid.at[t], shid_s.at[k - 1], shid_r.at[t], (f, (t + k) % Pn)).start()
    for k in range(1, Pn):
        arrived(shid.at[(t + k) % Pn], shid_r.at[(t + k) % Pn])

    def shared_out(n):
        at = pl.ds(pl.multiple_of(n * nt, nt), nt)
        total = None
        for q in range(Pn):
            w = sdb[q * per : (q + 1) * per, :, at].reshape(Sc, nt)
            term = jnp.dot(shid[q], w, preferred_element_type=F32)
            total = term if total is None else total + term
        acc[:, at] = total

    loop(Dc // nt, shared_out)

    def wait_gu(k):
        s = source(k)
        arrived(gub.at[s], gu_r.at[s])

    loop(E - 1, wait_gu)
    puts.append(put(gub.at[:, :, pl.ds(0, Hc)], eg, 4))
    puts.append(put(gub.at[:, :, pl.ds(Hc, Hc)], eu, 5))
    M, g, groups = S.M, S.g, S.groups
    own = f // g

    def group_at(k):
        return ring(k, groups, own) if groups > 1 else 0

    def hidden_in(k):
        q0 = group_at(k)
        span = pl.ds(q0 * g, g)
        total = None
        for q in range(Pn):
            w = gub[q * per : (q + 1) * per].reshape(Dc, 2 * Hc)
            term = jnp.dot(rows[q, span].reshape(M, Dc), w, preferred_element_type=F32)
            total = term if total is None else total + term
        hid[t, span] = act(total, Hc).reshape(g, cap, Hc)

    def send_hidden(k):
        span = pl.ds(group_at(k) * g, g)
        for j in range(1, Pn):
            tt = (t + j) % Pn
            rcopy(
                hid.at[t, span], hid.at[t, span], hid_s.at[j - 1], hid_r.at[t, k], (f, tt)
            ).start()

    def hidden_step(k):
        hidden_in(k)

        @pl.when(k > 0)
        def _():
            send_hidden(k - 1)

    loop(groups, hidden_step)

    def wait_dn(k):
        s = source(k)
        arrived(dnb.at[s], dn_r.at[s])

    send_hidden(groups - 1)
    loop(E - 1, wait_dn)
    puts.append(spread(dnb, ed, edo_s, edo_r, 6))

    def send_back(k):
        for i in range(g):
            s = group_at(k) * g + i

            @pl.when(s != f)
            def _():
                rcopy(res.at[s], ret.at[f], ret_s.at[s], ret_r.at[f], (s, t)).start()

    def back_step(k):
        span = pl.ds(group_at(k) * g, g)
        for j in range(1, Pn):
            tt = (t + j) % Pn
            arrived(hid.at[tt, span], hid_r.at[tt, k])

        def part(n):
            at = pl.ds(pl.multiple_of(n * nt, nt), nt)
            total = None
            for q in range(Pn):
                w = dnb[q * per : (q + 1) * per, :, at].reshape(Hc, nt)
                term = jnp.dot(hid[q, span].reshape(M, Hc), w, preferred_element_type=F32)
                total = term if total is None else total + term
            res[span, :, at] = total.astype(BF16).reshape(g, cap, nt)

        loop(Dc // nt, part)
        send_back(k)

    loop(groups, back_step)
    ret[f] = res[f]

    def slot_cols(k):
        return jnp.sum(jnp.where(cols_of[:, k : k + 1] == name_cols, count_cols, 0.0), axis=1, keepdims=True)

    name_cols = lax.broadcasted_iota(jnp.int32, (T, 128), 1).astype(F32)
    chosen_cols = ((cols_of[:, 0:1] == name_cols) | (cols_of[:, 1:2] == name_cols)).astype(F32)
    after = lax.broadcasted_iota(jnp.int32, (T, T), 0) > lax.broadcasted_iota(
        jnp.int32, (T, T), 1
    )
    count_cols = jnp.dot(
        after.astype(F32).astype(BF16), chosen_cols.astype(BF16), preferred_element_type=F32
    )
    target0 = cols_of[:, 0:1] * cap + slot_cols(0)
    target1 = cols_of[:, 1:2] * cap + slot_cols(1)
    w0, w1 = cols_of[:, 2:3], cols_of[:, 3:4]

    def combine(i):
        q0 = group_at(groups - 1 - i)
        for j in range(g):
            s = q0 * g + j

            @pl.when(s != f)
            def _():
                arrived(ret.at[s], ret_r.at[s])

        spot = (lax.broadcasted_iota(jnp.int32, (T, M), 1) + q0 * M).astype(F32)
        weigh = jnp.where(target0 == spot, w0, 0.0) + jnp.where(target1 == spot, w1, 0.0)
        weigh = weigh.astype(BF16)

        def part(n):
            at = pl.ds(pl.multiple_of(n * nt, nt), nt)
            block = ret[pl.ds(q0 * g, g), :, at].reshape(M, nt)
            total = acc[:, at] + jnp.dot(weigh, block, preferred_element_type=F32)
            acc[:, at] = total

        loop(Dc // nt, part)

    loop(groups, combine)
    outb[...] = acc[...].astype(BF16)
    puts.append(put(outb, mixed, 7))

    line_drain(tok, by_z, tok_s)
    line_drain(shb, by_f, sh_s)
    line_drain(sdb, by_f, sd_s)
    for i in range(1, Z):
        sent(info.at[z], info_s.at[i - 1])
    for j in range(1, Y):
        sent(shb.at[pl.ds(0, Z)], shy_s.at[j - 1])
        sent(sdb.at[pl.ds(0, Z)], sdy_s.at[j - 1])
        sent(yst.at[:, j - 1], y_s.at[j - 1])
    for i in range(1, C):
        sent(rows.at[t], x_s.at[i - 1])
    for i in range(C):
        sent(rows.at[t], part_s.at[i])
    loop(E - 1, lambda k: sent(gst.at[k], gu_s.at[k]))
    loop(E - 1, lambda k: sent(dst.at[k], dn_s.at[k]))
    for k in range(1, Pn):
        sent(shid.at[t], shid_s.at[k - 1])
        sent(hid.at[t], hid_s.at[k - 1])

    def drain_ret(k):
        s = source(k)
        sent(res.at[s], ret_s.at[s])

    loop(E - 1, drain_ret)
    spread_wait(sdb, sd, sdo_s, sdo_r)
    spread_wait(dnb, ed, edo_s, edo_r)
    for copy in puts:
        copy.wait()


def on_device(
    tokens, norm_gain, gate_train, up_train, down_train,
    shared_gate_train, shared_up_train, shared_down_train, route_expert, route_weight,
):
    S = Sizes(
        lax.axis_size("fs"), lax.axis_size("tp"), tokens.shape, gate_train.shape,
        down_train.shape, shared_gate_train.shape, shared_down_train.shape,
        route_expert.shape[1],
    )
    E, Pn, C, Z, Y = S.E, S.P, S.C, S.Z, S.Y
    T, D, cap, Dr, Hc, Hr, Dc, Sc, Sr, per = (
        S.T, S.D, S.cap, S.Dr, S.Hc, S.Hr, S.Dc, S.Sc, S.Sr, S.per
    )
    route = route_expert.astype(F32)
    columns = jnp.concatenate([route, route_weight], axis=1)
    dma = pltpu.SemaphoreType.DMA
    anywhere = pl.BlockSpec(memory_space=pl.ANY)
    inside = pl.BlockSpec(memory_space=pltpu.VMEM)
    far = max(1, Y - 1)
    scratch = [
        pltpu.VMEM((T, D), BF16),
        pltpu.VMEM((Z, T, Dc), BF16),
        pltpu.VMEM((Z, 8, T), F32),
        pltpu.VMEM((E, Dr, 2 * Sc), BF16),
        pltpu.VMEM((E, Sr, Dc), BF16),
        pltpu.VMEM((E, Dr, 2 * Hc), BF16),
        pltpu.VMEM((E, Dr, 2 * Hc), BF16),
        pltpu.VMEM((E, Hr, Dc), BF16),
        pltpu.VMEM((E, Hr, Dc), BF16),
        pltpu.VMEM((Pn, E, cap, Dc), BF16),
        pltpu.VMEM((Z, far, cap, Dc), BF16),
        pltpu.VMEM((Pn, E, cap, Hc), BF16),
        pltpu.VMEM((E, cap, Dc), BF16),
        pltpu.VMEM((E, cap, Dc), BF16),
        pltpu.VMEM((T, Dc), F32),
        pltpu.VMEM((Pn, T, Sc), BF16),
        pltpu.VMEM((T, Dc), BF16),
        pltpu.VMEM((2, 2, Dr, Hc), F32),
        pltpu.VMEM((2, Hr, Dc), F32),
        dma((2, 3)), dma((1,)), dma((8,)),
        dma((2, Z)), dma((Z,)), dma((Z,)), dma((Z,)),
        dma((2, Z)), dma((E,)), dma((far,)),
        dma((2, Z)), dma((E,)), dma((far,)),
        dma((E,)), dma((E,)), dma((E,)), dma((E,)),
        dma((far,)), dma((Pn, E)), dma((C,)), dma((C,)), dma((C,)),
        dma((Pn,)), dma((Pn, S.groups)), dma((Pn,)), dma((Pn,)),
        dma((Pn,)), dma((Pn,)), dma((Pn,)), dma((Pn,)),
        dma((E,)), dma((E,)),
    ]
    shape = lambda *dims: jax.ShapeDtypeStruct(dims, BF16)
    flops = 2 * T * D * 2 * Sc + 2 * E * cap * D * 2 * Hc + 4 * E * cap * D * Hc
    outs = pl.pallas_call(
        functools.partial(kernel, S),
        out_shape=[
            shape(E, Dr, Hc), shape(E, Dr, Hc), shape(per, Hr, D),
            shape(E, Dr, Sc), shape(E, Dr, Sc), shape(per, Sr, D), shape(T, Dc),
        ],
        in_specs=[anywhere] * 7 + [inside] * 3,
        out_specs=[anywhere] * 7,
        scratch_shapes=scratch,
        compiler_params=pltpu.CompilerParams(
            has_side_effects=True, vmem_limit_bytes=67043328
        ),
        cost_estimate=pl.CostEstimate(flops=flops, bytes_accessed=1 << 26, transcendentals=0),
    )(
        tokens, gate_train, up_train, down_train, shared_gate_train, shared_up_train,
        shared_down_train, norm_gain[:, None], route.T, columns,
    )
    eg, eu, ed, sg, su, sd, mixed = outs
    return (
        eg.reshape(1, D, Hc), eu.reshape(1, D, Hc), ed.reshape(1, per * Hr, D),
        sg.reshape(D, Sc), su.reshape(D, Sc), sd.reshape(per * Sr, D), mixed,
    )


def solution(mesh):
    placed = (
        P("fs", None),
        P("fs"),
        P(None, "fs", "tp"),
        P(None, "fs", "tp"),
        P(None, "fs", "tp"),
        P("fs", "tp"),
        P("fs", "tp"),
        P("fs", "tp"),
        P("fs", None),
        P("fs", None),
    )
    return jax.shard_map(
        on_device,
        mesh=mesh,
        in_specs=placed,
        out_specs=(
            P("fs", None, "tp"),
            P("fs", None, "tp"),
            P("fs", "tp", None),
            P(None, "tp"),
            P(None, "tp"),
            P("tp", None),
            P("fs", "tp"),
        ),
        check_vma=False,
    )
```

profile of v0, /device:TPU:20, one launch (start us, length us, event | category | flops | bytes accessed | tf_op | source)
XLA Modules:
  0.0 406.4 jit_solution(12649067465585081597)
XLA Ops:
  0.6 1.3 fusion
  1.9 0.7 pad_maximum_fusion
  2.6 0.9 copy.25.cols_of
  3.5 1.5 copy.24.gain
  5.0 385.9 %shard_map.153 = (bf16[8,512,256]{2,1,0:T(8,128)(2,1)}, bf16[8,512,256]{2,1,0:T(8,128)(2,1)}, bf16[2,128,4096]{2,1,0:T(8,128)(2,1)}, bf16[8,512,256]{2,1,0:T(8,1...) custom-call(bf16[512,4096]{1,0:T(8,128)(2,1)} %tokens.1, ...), custom_call_target="tpu_custom_call" | custom-call | flops 15032385536 | bytes 67108864 | tf_op jit(solution)/shard_map/pallas_call | solution.py:567
  390.9 0.0 copy-start.4
  390.9 3.2 copy.33
  394.1 0.0 copy-done.4
  394.1 0.0 copy-start.3
  394.1 1.3 copy.34
  395.4 1.0 copy-done.3
  396.5 0.0 copy-start.2
  396.5 1.3 copy.35
  397.8 1.0 copy-done.2
  398.8 0.0 copy-start.1
  398.8 1.3 copy.36
  400.1 1.0 copy-done.1
  401.1 0.0 copy-start
  401.2 1.3 copy.37
  402.5 1.0 copy-done
  403.5 0.0 copy-start.5
  403.5 1.3 copy.38
  404.8 0.6 copy-done.5
  405.5 1.0 copy.39
Async XLA Ops:
  390.9 3.2 copy-start.4
  394.1 2.3 copy-start.3
  396.5 2.3 copy-start.2
  398.8 2.3 copy-start.1
  401.1 2.3 copy-start
  403.5 2.0 copy-start.5
where the time goes:
time: 411 us; the launch traced here: 406 us
  Pallas kernels  386 us (94%)
  local copies, waits for them, and re-layouts  17.9 us (4%)
    pallas_call x1, Pallas kernels, on_device(): pl.pallas_call(functools.partial(kernel, S), out_shape=[shape(E, Dr, Hc),...  386 us
    unnamed x19, local copies, waits for them, and re-layouts  15.5 us

commit v1 on v0

--- a/solution.py
+++ b/solution.py
@@ -39,13 +39,13 @@
 
 def kernel(
     S,
-    tokens, gate_t, up_t, down_t, sgate_t, sup_t, sdown_t, gain, rows_of, cols_of,
+    tokens, gate_t, up_t, down_t, sgate_t, sup_t, sdown_t, gain, route, weight,
     eg, eu, ed, sg, su, sd, mixed,
-    nrm, tok, info, shb, sdb, gst, gub, dst, dnb, rows, yst, hid, res, ret, acc, shid, outb,
-    wbuf, dbuf,
+    nrm, tok, info, shb, sdb, gst, gub, dst, dnb, rows, yst, est, hid, res, ret, acc, shid, outb,
+    wbuf, dbuf, gcol,
     ld_sem, tk_ld, out_sem,
     tok_s, tok_r, info_s, info_r, sh_s, sh_r, shy_s, sd_s, sd_r, sdy_s,
-    gu_s, gu_r, dn_s, dn_r, y_s, rows_r, x_s, part_s, part_r,
+    gu_s, gu_r, dn_s, dn_r, y_s, e_s, rows_r, x_s, part_s, part_r,
     hid_s, hid_r, shid_s, shid_r, edo_s, edo_r, sdo_s, sdo_r, ret_s, ret_r,
 ):
     E, Pn, C, Z, Y, half, per = S.E, S.P, S.C, S.Z, S.Y, S.half, S.per
@@ -53,7 +53,8 @@
     f, t = lax.axis_index("fs"), lax.axis_index("tp")
     z, y = f // Y, f % Y
     x, c = t // cores, t % cores
-    h, fo = f // half, f % half
+    inner = (z > 0) & (z < Z - 1)
+    to_low, to_high = z == 1, z == Z - 2
 
     def ring(k, count, at, back=False):
         mid = count // 2
@@ -103,10 +104,20 @@
     ]
     for copy in sh_loads + load_w(0, 0) + [load_d(0, 0)]:
         copy.start()
+    greet = pltpu.get_barrier_semaphore()
+    for i in range(1, E):
+        pl.semaphore_signal(greet, inc=1, device_id=((f + i) % E, t), device_id_type=MESH)
+    for i in range(1, Pn):
+        pl.semaphore_signal(greet, inc=1, device_id=(f, (t + i) % Pn), device_id_type=MESH)
 
     T = S.T
     wide = max(16, E)
-    r0, r1 = rows_of[0:1, :], rows_of[1:2, :]
+    gcol[...] = jnp.broadcast_to(gain[...], (128, S.Dr)).T
+    lanes = lax.broadcasted_iota(jnp.int32, (T, 128), 1)
+    routes = route[...].astype(F32)
+    named0, named1 = routes[:, 0:1], routes[:, 1:2]
+    by_row = jnp.where(lanes == 0, named0, named1).T
+    r0, r1 = by_row[0:1, :], by_row[1:2, :]
     names = lax.broadcasted_iota(jnp.int32, (wide, T), 0).astype(F32)
     hit0, hit1 = r0 == names, r1 == names
     chosen = (hit0 | hit1).astype(F32).astype(BF16)
@@ -135,46 +146,60 @@
 
     for copy in sh_loads:
         copy.wait()
-    shb[f, :, 0:Sc] = (gain[...] * wbuf[1, 0]).astype(BF16)
-    shb[f, :, Sc:] = (gain[...] * wbuf[1, 1]).astype(BF16)
+    shb[f, :, 0:Sc] = (gcol[:, 0:1] * wbuf[1, 0]).astype(BF16)
+    shb[f, :, Sc:] = (gcol[:, 0:1] * wbuf[1, 1]).astype(BF16)
     sdb[f] = dbuf[1].astype(BF16)
 
-    def line(buf, slot_of, ssem, rsem, hop):
-        for d, ok_next in ((0, z + 1 < Z), (1, z > 0)):
+    by_z = lambda zs: zs
+    by_f = lambda zs: zs * Y + y
+
+    pl.semaphore_wait(greet, E + Pn - 2)
+
+    def lanes_of(slot_of, hop, within):
+        low, high = (1, Z - 1) if within else (0, Z)
+        for d in range(2):
             zs = z - hop if d == 0 else z + hop
             there = (zs >= 0) if d == 0 else (zs < Z)
-            slot = slot_of(jnp.clip(zs, 0, Z - 1))
-            nxt = (f + Y if d == 0 else f - Y, t)
+            if within and hop:
+                there &= inner
+            onward = (z + 1 < high) if d == 0 else (z > low)
+            yield d, there, onward, slot_of(jnp.clip(zs, 0, Z - 1)), f + Y if d == 0 else f - Y
+
+    def line(buf, slot_of, ssem, rsem, hop, within=False):
+        for d, there, onward, slot, nxt in lanes_of(slot_of, hop, within):
 
             @pl.when(there)
             def _():
                 if hop:
                     arrived(buf.at[slot], rsem.at[slot])
 
-                @pl.when(ok_next)
+                @pl.when(onward)
                 def _():
                     rcopy(
-                        buf.at[slot], buf.at[slot], ssem.at[d, hop], rsem.at[slot], nxt
+                        buf.at[slot], buf.at[slot], ssem.at[d, hop], rsem.at[slot], (nxt, t)
                     ).start()
 
-    def line_drain(buf, slot_of, ssem):
-        for hop in range(Z - 1):
-            for d, ok_next in ((0, z + 1 < Z), (1, z > 0)):
-                zs = z - hop if d == 0 else z + hop
-                there = (zs >= 0) if d == 0 else (zs < Z)
-                slot = slot_of(jnp.clip(zs, 0, Z - 1))
-
-                @pl.when(there & ok_next)
-                def _():
-                    sent(buf.at[slot], ssem.at[d, hop])
-
-    by_z = lambda zs: zs
-    by_f = lambda zs: zs * Y + y
-
-    for i in range(1, Z):
-        zo = (z + i) % Z
-        rcopy(info.at[z], info.at[z], info_s.at[i - 1], info_r.at[z], (zo * Y + y, t)).start()
-    line(tok, by_z, tok_s, tok_r, 0)
+    def line_sent(buf, slot_of, ssem, hop, within=False):
+        for d, there, onward, slot, nxt in lanes_of(slot_of, hop, within):
+
+            @pl.when(there & onward)
+            def _():
+                sent(buf.at[slot], ssem.at[d, hop])
+
+    def tell(act_on):
+        for i in range(1, Z):
+            zo = (z + i) % Z
+
+            @pl.when((zo > 0) & (zo < Z - 1))
+            def _():
+                act_on(i - 1, zo)
+
+    tell(
+        lambda i, zo: rcopy(
+            info.at[z], info.at[z], info_s.at[i], info_r.at[z], (zo * Y + y, t)
+        ).start()
+    )
+    line(tok, by_z, tok_s, tok_r, 0, True)
 
     def convert_gu(k):
         slot = k % 2
@@ -187,7 +212,7 @@
                 copy.start()
 
         for i in range(2):
-            gst[k, :, i * Hc : (i + 1) * Hc] = (gain[...] * wbuf[slot, i]).astype(BF16)
+            gst[k, :, i * Hc : (i + 1) * Hc] = (gcol[:, 0:1] * wbuf[slot, i]).astype(BF16)
 
     def convert_dn(k):
         slot = k % 2
@@ -198,8 +223,6 @@
             load_d(k + 1, 1 - slot).start()
 
         dst[k] = dbuf[slot].astype(BF16)
-
-    loop(E, convert_gu)
 
     def shared_y(zs):
         s = by_f(zs)
@@ -208,37 +231,56 @@
             rcopy(shb.at[s], shb.at[s], shy_s.at[j - 1], sh_r.at[s], to).start()
             rcopy(sdb.at[s], sdb.at[s], sdy_s.at[j - 1], sd_r.at[s], to).start()
 
-    line(shb, by_f, sh_s, sh_r, 0)
-    line(sdb, by_f, sd_s, sd_r, 0)
-    shared_y(z)
-    loop(E, convert_dn)
-    gub[f] = gst[E - 1]
-    dnb[f] = dst[E - 1]
-
     def x_out(s):
         for i in range(1, C):
             to = (f, (x + i) % C * cores + c)
             rcopy(rows.at[t, s], rows.at[t, s], x_s.at[i - 1], rows_r.at[t, s], to).start()
         rcopy(rows.at[t, s], rows.at[t, s], part_s.at[0], part_r.at[0], (f, x * cores + 1 - c)).start()
 
+    def picked(zs, e, put_block):
+        e = e.astype(F32)
+        slots = lax.broadcasted_iota(jnp.int32, (cap, T), 0).astype(F32)
+        got = (info[zs, 0:1, :] == e) & (info[zs, 2:3, :] == slots)
+        got |= (info[zs, 1:2, :] == e) & (info[zs, 3:4, :] == slots)
+        got = got.astype(F32).astype(BF16)
+
+        def part(n):
+            at = pl.ds(pl.multiple_of(n * nt, nt), nt)
+            put_block(at, jnp.dot(got, tok[zs, :, at], preferred_element_type=F32).astype(BF16))
+
+        loop(Dc // nt, part)
+
     def pick(zs):
         s = by_f(zs)
+
+        def for_end(zt):
+            for j in range(Y):
+
+                def put_block(at, block):
+                    est[zs, j, :, at] = block
+
+                picked(zs, zt * Y + (y + j) % Y, put_block)
+            for j in range(Y):
+                rcopy(
+                    est.at[zs, j], rows.at[t, s], e_s.at[j], rows_r.at[t, s],
+                    (zt * Y + (y + j) % Y, t),
+                ).start()
+
+        for zt, near in ((0, to_low), (Z - 1, to_high)):
+
+            @pl.when(near & (zs != zt))
+            def _():
+                for_end(zt)
+
         for j in list(range(1, Y)) + [0]:
-            e = (z * Y + (y + j) % Y).astype(F32)
-            slots = lax.broadcasted_iota(jnp.int32, (cap, T), 0).astype(F32)
-            got = (info[zs, 0:1, :] == e) & (info[zs, 2:3, :] == slots)
-            got |= (info[zs, 1:2, :] == e) & (info[zs, 3:4, :] == slots)
-            got = got.astype(F32).astype(BF16)
-
-            def part(n):
-                at = pl.ds(pl.multiple_of(n * nt, nt), nt)
-                block = jnp.dot(got, tok[zs, :, at], preferred_element_type=F32).astype(BF16)
+
+            def put_block(at, block):
                 if j:
                     yst[zs, j - 1, :, at] = block
                 else:
                     rows[t, s, :, at] = block
 
-            loop(Dc // nt, part)
+            picked(zs, z * Y + (y + j) % Y, put_block)
         for j in range(1, Y):
             to = (z * Y + (y + j) % Y, t)
             rcopy(
@@ -246,8 +288,6 @@
             ).start()
         x_out(s)
 
-    pick(z)
-
     def send_gu(k):
         e = peer(k)
         rcopy(gst.at[k], gub.at[f], gu_s.at[k], gu_r.at[f], (e, t)).start()
@@ -256,32 +296,70 @@
         e = peer(k)
         rcopy(dst.at[k], dnb.at[f], dn_s.at[k], dn_r.at[f], (e, t)).start()
 
-    def arrivals(hop):
+    def come(hop, act_on):
         for zs, there in ((z - hop, z - hop >= 0), (z + hop, z + hop < Z)):
             at = jnp.clip(zs, 0, Z - 1)
 
             @pl.when(there)
             def _():
-                shared_y(at)
-                arrived(info.at[at], info_r.at[at])
-                pick(at)
-
-    for hop in range(1, Z):
-        line(tok, by_z, tok_s, tok_r, hop)
+                act_on(at)
+
+    def pick_come(at):
+        arrived(info.at[at], info_r.at[at])
+        pick(at)
+
+    def tok_hop(hop):
+        line(tok, by_z, tok_s, tok_r, hop, True)
+
+        @pl.when(inner)
+        def _():
+            come(hop, pick_come)
+
+    def shared_hop(hop):
         line(shb, by_f, sh_s, sh_r, hop)
         line(sdb, by_f, sd_s, sd_r, hop)
-        if hop == 1:
-            loop(half, send_gu)
-        if hop == Z - 2 or Z <= 2:
-            loop(E - 1, send_gu, half)
-            loop(E - 1, send_dn)
-        arrivals(hop)
-
-    for j in range(1, Y):
-        for zs in range(Z):
+        if hop:
+            come(hop, shared_y)
+        else:
+            shared_y(z)
+
+    pick(z)
+    loop(E, convert_gu)
+    loop(E, convert_dn)
+    gub[f] = gst[E - 1]
+    dnb[f] = dst[E - 1]
+    if Z > 2:
+        tok_hop(1)
+    line_sent(tok, by_z, tok_s, 0, True)
+    if Z > 2:
+        line_sent(tok, by_z, tok_s, 1, True)
+    shared_hop(0)
+    for hop in range(2, Z - 1):
+        tok_hop(hop)
+    shared_hop(1)
+    line_sent(shb, by_f, sh_s, 0)
+    line_sent(sdb, by_f, sd_s, 0)
+    loop(half // 2, send_gu)
+    loop(E - 1, send_gu, half)
+
+    for i in range(Z):
+        zs = jnp.where(z < Z // 2, z + i, z + Z - i) % Z
+        for j in range(Y):
             s = zs * Y + (y + j) % Y
-            arrived(rows.at[t, s], rows_r.at[t, s])
-            x_out(s)
+            if j:
+                arrived(rows.at[t, s], rows_r.at[t, s])
+                x_out(s)
+            elif i:
+
+                @pl.when(jnp.logical_not(inner))
+                def _():
+                    arrived(rows.at[t, s], rows_r.at[t, s])
+                    x_out(s)
+
+    for hop in range(2, Z - 1):
+        shared_hop(hop)
+    loop(half // 2, lambda k: sent(gst.at[k], gu_s.at[k]))
+    loop(half, send_gu, half // 2)
     for i in range(1, C):
         to_t = (x + i) % C * cores + c
 
@@ -293,19 +371,15 @@
             ).start()
 
         loop(E, forward)
-
-    for j in range(1, Y):
-        for zs in range(Z):
-            s = zs * Y + (y + j) % Y
-            arrived(shb.at[s], sh_r.at[s])
-            arrived(sdb.at[s], sd_r.at[s])
+    loop(half, lambda k: sent(gst.at[k], gu_s.at[k]), half // 2)
+    loop(E - 1, send_dn)
 
     def put(src, dst_ref, i):
         copy = pltpu.make_async_copy(src, dst_ref, out_sem.at[i])
         copy.start()
         return copy
 
-    puts = [put(shb.at[:, :, pl.ds(0, Sc)], sg, 1), put(shb.at[:, :, pl.ds(Sc, Sc)], su, 2)]
+    puts = []
     own_cols = pl.ds(pl.multiple_of(t * Dc, Dc), Dc)
 
     def spread(buf, out, ssem, rsem, i):
@@ -324,8 +398,6 @@
             at = pl.ds(pl.multiple_of(tt * Dc, Dc), Dc)
             arrived(out.at[:, :, at], rsem.at[tt])
 
-    puts.append(spread(sdb, sd, sdo_s, sdo_r, 3))
-
     def act(v, width):
         gate, up = v[:, :width], v[:, width:]
         return (gate / (1.0 + jnp.exp(-gate)) * up).astype(BF16)
@@ -341,8 +413,6 @@
             total = term if total is None else total + term
         shid[t, at, :] = act(total, Sc)
 
-    loop(T // mt, shared_in)
-
     def rows_waits():
         part = x * cores + 1 - c
         arrived(rows.at[part], part_r.at[0])
@@ -350,21 +420,6 @@
             arrived(rows.at[(x + i) % C * cores + 1 - c], part_r.at[i])
 
     rows_waits()
-    for k in range(1, Pn):
-        rcopy(shid.at[t], shid.at[t], shid_s.at[k - 1], shid_r.at[t], (f, (t + k) % Pn)).start()
-    for k in range(1, Pn):
-        arrived(shid.at[(t + k) % Pn], shid_r.at[(t + k) % Pn])
-
-    def shared_out(n):
-        at = pl.ds(pl.multiple_of(n * nt, nt), nt)
-        total = None
-        for q in range(Pn):
-            w = sdb[q * per : (q + 1) * per, :, at].reshape(Sc, nt)
-            term = jnp.dot(shid[q], w, preferred_element_type=F32)
-            total = term if total is None else total + term
-        acc[:, at] = total
-
-    loop(Dc // nt, shared_out)
 
     def wait_gu(k):
         s = source(k)
@@ -411,6 +466,8 @@
         arrived(dnb.at[s], dn_r.at[s])
 
     send_hidden(groups - 1)
+    if Z > 2:
+        shared_hop(Z - 1)
     loop(E - 1, wait_dn)
     puts.append(spread(dnb, ed, edo_s, edo_r, 6))
 
@@ -443,20 +500,47 @@
     loop(groups, back_step)
     ret[f] = res[f]
 
-    def slot_cols(k):
-        return jnp.sum(jnp.where(cols_of[:, k : k + 1] == name_cols, count_cols, 0.0), axis=1, keepdims=True)
-
+    for j in range(1, Y):
+        for zs in range(Z):
+            s = zs * Y + (y + j) % Y
+            arrived(shb.at[s], sh_r.at[s])
+            arrived(sdb.at[s], sd_r.at[s])
+
+    puts += [put(shb.at[:, :, pl.ds(0, Sc)], sg, 1), put(shb.at[:, :, pl.ds(Sc, Sc)], su, 2)]
+    loop(T // mt, shared_in)
+
+    for k in range(1, Pn):
+        rcopy(shid.at[t], shid.at[t], shid_s.at[k - 1], shid_r.at[t], (f, (t + k) % Pn)).start()
+    for k in range(1, Pn):
+        arrived(shid.at[(t + k) % Pn], shid_r.at[(t + k) % Pn])
+
+    def shared_out(n):
+        at = pl.ds(pl.multiple_of(n * nt, nt), nt)
+        total = None
+        for q in range(Pn):
+            w = sdb[q * per : (q + 1) * per, :, at].reshape(Sc, nt)
+            term = jnp.dot(shid[q], w, preferred_element_type=F32)
+            total = term if total is None else total + term
+        acc[:, at] = total
+
+    loop(Dc // nt, shared_out)
+
+    puts.append(spread(sdb, sd, sdo_s, sdo_r, 3))
+
+    routes = route[...].astype(F32)
+    named0, named1 = routes[:, 0:1], routes[:, 1:2]
     name_cols = lax.broadcasted_iota(jnp.int32, (T, 128), 1).astype(F32)
-    chosen_cols = ((cols_of[:, 0:1] == name_cols) | (cols_of[:, 1:2] == name_cols)).astype(F32)
+    is0, is1 = named0 == name_cols, named1 == name_cols
+    chosen_cols = (is0 | is1).astype(F32)
     after = lax.broadcasted_iota(jnp.int32, (T, T), 0) > lax.broadcasted_iota(
         jnp.int32, (T, T), 1
     )
     count_cols = jnp.dot(
         after.astype(F32).astype(BF16), chosen_cols.astype(BF16), preferred_element_type=F32
     )
-    target0 = cols_of[:, 0:1] * cap + slot_cols(0)
-    target1 = cols_of[:, 1:2] * cap + slot_cols(1)
-    w0, w1 = cols_of[:, 2:3], cols_of[:, 3:4]
+    target0 = named0 * cap + jnp.sum(jnp.where(is0, count_cols, 0.0), axis=1, keepdims=True)
+    target1 = named1 * cap + jnp.sum(jnp.where(is1, count_cols, 0.0), axis=1, keepdims=True)
+    w0, w1 = weight[:, 0:1], weight[:, 1:2]
 
     def combine(i):
         q0 = group_at(groups - 1 - i)
@@ -483,20 +567,34 @@
     outb[...] = acc[...].astype(BF16)
     puts.append(put(outb, mixed, 7))
 
-    line_drain(tok, by_z, tok_s)
-    line_drain(shb, by_f, sh_s)
-    line_drain(sdb, by_f, sd_s)
-    for i in range(1, Z):
-        sent(info.at[z], info_s.at[i - 1])
+    for hop in range(1, Z - 1):
+        if hop > 1:
+            line_sent(tok, by_z, tok_s, hop, True)
+        line_sent(shb, by_f, sh_s, hop)
+        line_sent(sdb, by_f, sd_s, hop)
+    tell(lambda i, zo: sent(info.at[z], info_s.at[i]))
     for j in range(1, Y):
         sent(shb.at[pl.ds(0, Z)], shy_s.at[j - 1])
         sent(sdb.at[pl.ds(0, Z)], sdy_s.at[j - 1])
-        sent(yst.at[:, j - 1], y_s.at[j - 1])
+
+        @pl.when(inner)
+        def _():
+            sent(yst.at[:, j - 1], y_s.at[j - 1])
+
+        @pl.when(jnp.logical_not(inner))
+        def _():
+            sent(yst.at[0, j - 1], y_s.at[j - 1])
+
+    @pl.when(to_low | to_high)
+    def _():
+        for j in range(Y):
+            sent(est.at[pl.ds(0, Z - 1), j], e_s.at[j])
+
     for i in range(1, C):
         sent(rows.at[t], x_s.at[i - 1])
     for i in range(C):
         sent(rows.at[t], part_s.at[i])
-    loop(E - 1, lambda k: sent(gst.at[k], gu_s.at[k]))
+    loop(E - 1, lambda k: sent(gst.at[k], gu_s.at[k]), half)
     loop(E - 1, lambda k: sent(dst.at[k], dn_s.at[k]))
     for k in range(1, Pn):
         sent(shid.at[t], shid_s.at[k - 1])
@@ -511,6 +609,30 @@
     spread_wait(dnb, ed, edo_s, edo_r)
     for copy in puts:
         copy.wait()
+
+
+def handed(count, parts, *refs):
+    ins, outs, held = refs[:count], refs[count : 2 * count], refs[2 * count : 3 * count]
+    in_sem, out_sem = refs[3 * count :]
+
+    def piece(i, j, ref):
+        rows = ref.shape[0] // parts
+        return ref.at[pl.ds(j * rows, rows)]
+
+    def taken(i, j):
+        return pltpu.make_async_copy(piece(i, j, ins[i]), piece(i, j, held[i]), in_sem.at[i, j])
+
+    def given(i, j):
+        return pltpu.make_async_copy(piece(i, j, held[i]), piece(i, j, outs[i]), out_sem.at[i, j])
+
+    every = [(i, j) for i in range(count) for j in range(parts)]
+    for at in every:
+        taken(*at).start()
+    for at in every:
+        taken(*at).wait()
+        given(*at).start()
+    for at in every:
+        given(*at).wait()
 
 
 def on_device(
@@ -526,8 +648,6 @@
     T, D, cap, Dr, Hc, Hr, Dc, Sc, Sr, per = (
         S.T, S.D, S.cap, S.Dr, S.Hc, S.Hr, S.Dc, S.Sc, S.Sr, S.per
     )
-    route = route_expert.astype(F32)
-    columns = jnp.concatenate([route, route_weight], axis=1)
     dma = pltpu.SemaphoreType.DMA
     anywhere = pl.BlockSpec(memory_space=pl.ANY)
     inside = pl.BlockSpec(memory_space=pltpu.VMEM)
@@ -544,6 +664,7 @@
         pltpu.VMEM((E, Hr, Dc), BF16),
         pltpu.VMEM((Pn, E, cap, Dc), BF16),
         pltpu.VMEM((Z, far, cap, Dc), BF16),
+        pltpu.VMEM((Z, Y, cap, Dc), BF16),
         pltpu.VMEM((Pn, E, cap, Hc), BF16),
         pltpu.VMEM((E, cap, Dc), BF16),
         pltpu.VMEM((E, cap, Dc), BF16),
@@ -552,12 +673,13 @@
         pltpu.VMEM((T, Dc), BF16),
         pltpu.VMEM((2, 2, Dr, Hc), F32),
         pltpu.VMEM((2, Hr, Dc), F32),
+        pltpu.VMEM((Dr, 128), F32),
         dma((2, 3)), dma((1,)), dma((8,)),
         dma((2, Z)), dma((Z,)), dma((Z,)), dma((Z,)),
         dma((2, Z)), dma((E,)), dma((far,)),
         dma((2, Z)), dma((E,)), dma((far,)),
         dma((E,)), dma((E,)), dma((E,)), dma((E,)),
-        dma((far,)), dma((Pn, E)), dma((C,)), dma((C,)), dma((C,)),
+        dma((far,)), dma((Y,)), dma((Pn, E)), dma((C,)), dma((C,)), dma((C,)),
         dma((Pn,)), dma((Pn, S.groups)), dma((Pn,)), dma((Pn,)),
         dma((Pn,)), dma((Pn,)), dma((Pn,)), dma((Pn,)),
         dma((E,)), dma((E,)),
@@ -574,14 +696,24 @@
         out_specs=[anywhere] * 7,
         scratch_shapes=scratch,
         compiler_params=pltpu.CompilerParams(
-            has_side_effects=True, vmem_limit_bytes=67043328
+            collective_id=0, has_side_effects=True, vmem_limit_bytes=67043328
         ),
         cost_estimate=pl.CostEstimate(flops=flops, bytes_accessed=1 << 26, transcendentals=0),
     )(
         tokens, gate_train, up_train, down_train, shared_gate_train, shared_up_train,
-        shared_down_train, norm_gain[:, None], route.T, columns,
-    )
-    eg, eu, ed, sg, su, sd, mixed = outs
+        shared_down_train, norm_gain[None, :], route_expert, route_weight,
+    )
+    parts = 2
+    in_hbm = pl.BlockSpec(memory_space=pl.ANY)
+    eg, eu, ed, sg, su, sd, mixed = pl.pallas_call(
+        functools.partial(handed, len(outs), parts),
+        out_shape=[jax.ShapeDtypeStruct(o.shape, o.dtype) for o in outs],
+        in_specs=[in_hbm] * len(outs),
+        out_specs=[in_hbm] * len(outs),
+        scratch_shapes=[pltpu.VMEM(o.shape, o.dtype) for o in outs]
+        + [dma((len(outs), parts))] * 2,
+        compiler_params=pltpu.CompilerParams(vmem_limit_bytes=62 << 20),
+    )(*outs)
     return (
         eg.reshape(1, D, Hc), eu.reshape(1, D, Hc), ed.reshape(1, per * Hr, D),
         sg.reshape(D, Sc), su.reshape(D, Sc), sd.reshape(per * Sr, D), mixed,

time: 411 us -> 326 us (0.79)
  the two profiles are of different devices: /device:TPU:20 before, /device:TPU:1 now
where the time goes in v1:
time: 326 us
  Pallas kernels  322 us (99%)
    pallas_call x1, Pallas kernels, on_device(): pl.pallas_call(functools.partial(kernel, S), out_shape=[shape(E, Dr, Hc),...  312 us
    pallas_call x1, Pallas kernels, on_device(): pl.pallas_call(functools.partial(handed, len(outs), parts), out_shape=[ja...  9.72 us

profile of v1, /device:TPU:1, one launch (start us, length us, event | category | flops | bytes accessed | tf_op | source)
XLA Modules:
  0.0 325.6 jit_solution(12089598750702152090)
XLA Ops:
  0.6 1.5 copy.17.route
  2.2 1.5 copy.18.weight
  3.7 312.0 %shard_map.153 = (bf16[8,512,256]{2,1,0:T(8,128)(2,1)}, bf16[8,512,256]{2,1,0:T(8,128)(2,1)}, bf16[2,128,4096]{2,1,0:T(8,128)(2,1)}, bf16[8,512,256]{2,1,0:T(8,1...) custom-call(bf16[512,4096]{1,0:T(8,128)(2,1)} %tokens.1, ...), custom_call_target="tpu_custom_call" | custom-call | flops 15032385536 | bytes 67108864 | tf_op jit(solution)/shard_map/pallas_call | solution.py:689
  315.8 9.7 %shard_map.154 = (bf16[8,512,256]{2,1,0:T(8,128)(2,1)}, bf16[8,512,256]{2,1,0:T(8,128)(2,1)}, bf16[2,128,4096]{2,1,0:T(8,128)(2,1)}, bf16[8,512,256]{2,1,0:T(8,1...) custom-call(bf16[8,512,256]{2,1,0:T(8,128)(2,1)} %get-tuple-element.21.refs_0_, ...), custom_call_target="tpu_custom_call" | custom-call | tf_op jit(solution)/shard_map/pallas_call | solution.py:708

commit v2 on v1

--- a/solution.py
+++ b/solution.py
@@ -41,12 +41,13 @@
     S,
     tokens, gate_t, up_t, down_t, sgate_t, sup_t, sdown_t, gain, route, weight,
     eg, eu, ed, sg, su, sd, mixed,
-    nrm, tok, info, shb, sdb, gst, gub, dst, dnb, rows, yst, est, hid, res, ret, acc, shid, outb,
+    nrm, tok, info, shb, sdb, gst, gub, dst, dnb, rows, yst, est, hid, res, ret, cmb, farin, acc, shid, outb,
     wbuf, dbuf, gcol,
     ld_sem, tk_ld, out_sem,
     tok_s, tok_r, info_s, info_r, sh_s, sh_r, shy_s, sd_s, sd_r, sdy_s,
     gu_s, gu_r, dn_s, dn_r, y_s, e_s, rows_r, x_s, part_s, part_r,
     hid_s, hid_r, shid_s, shid_r, edo_s, edo_r, sdo_s, sdo_r, ret_s, ret_r,
+    cmb_r, far_s, far_r,
 ):
     E, Pn, C, Z, Y, half, per = S.E, S.P, S.C, S.Z, S.Y, S.half, S.per
     cap, Dc, Hc, Sc, nt = S.cap, S.Dc, S.Hc, S.Sc, S.nt
@@ -56,19 +57,12 @@
     inner = (z > 0) & (z < Z - 1)
     to_low, to_high = z == 1, z == Z - 2
 
-    def ring(k, count, at, back=False):
-        mid = count // 2
-        far = k // mid
-        off = k % mid + far
-        side = (at // mid + 1 + far) % 2
-        step = at % mid - off + count if back else at % mid + off
-        return side * mid + step % mid
-
     def peer(k):
-        return ring(k, E, f)
-
-    def source(k):
-        return ring(k, E, f, True)
+        span = Z // 2
+        p = k // Y
+        near = p // span
+        plane = (z // span + 1 + near) % 2 * span + (z + p + near) % span
+        return plane * Y + (y + 1 + k % Y) % Y
 
     def rcopy(src, dst, ssem, rsem, to):
         return pltpu.make_async_remote_copy(
@@ -111,13 +105,75 @@
         pl.semaphore_signal(greet, inc=1, device_id=(f, (t + i) % Pn), device_id_type=MESH)
 
     T = S.T
+    gcol[...] = jnp.broadcast_to(gain[...], (128, S.Dr)).T
+    for copy in sh_loads:
+        copy.wait()
+    shb[f, :, 0:Sc] = (gcol[:, 0:1] * wbuf[1, 0]).astype(BF16)
+    shb[f, :, Sc:] = (gcol[:, 0:1] * wbuf[1, 1]).astype(BF16)
+    sdb[f] = dbuf[1].astype(BF16)
+
+    by_z = lambda zs: zs
+    by_f = lambda zs: zs * Y + y
+
+    def lanes_of(slot_of, hop, within):
+        low, high = (1, Z - 1) if within else (0, Z)
+        for d in range(2):
+            zs = z - hop if d == 0 else z + hop
+            there = (zs >= 0) if d == 0 else (zs < Z)
+            if within and hop:
+                there &= inner
+            onward = (z + 1 < high) if d == 0 else (z > low)
+            yield d, there, onward, slot_of(jnp.clip(zs, 0, Z - 1)), f + Y if d == 0 else f - Y
+
+    def line(buf, slot_of, ssem, rsem, hop, within=False):
+        for d, there, onward, slot, nxt in lanes_of(slot_of, hop, within):
+
+            @pl.when(there)
+            def _():
+                if hop:
+                    arrived(buf.at[slot], rsem.at[slot])
+
+                @pl.when(onward)
+                def _():
+                    rcopy(
+                        buf.at[slot], buf.at[slot], ssem.at[d, hop], rsem.at[slot], (nxt, t)
+                    ).start()
+
+    def line_sent(buf, slot_of, ssem, hop, within=False):
+        for d, there, onward, slot, nxt in lanes_of(slot_of, hop, within):
+
+            @pl.when(there & onward)
+            def _():
+                sent(buf.at[slot], ssem.at[d, hop])
+
+
+    def shared_y(zs):
+        s = by_f(zs)
+        for j in range(1, Y):
+            to = (z * Y + (y + j) % Y, t)
+            rcopy(shb.at[s], shb.at[s], shy_s.at[j - 1], sh_r.at[s], to).start()
+            rcopy(sdb.at[s], sdb.at[s], sdy_s.at[j - 1], sd_r.at[s], to).start()
+
+    def come(hop, act_on):
+        for zs, there in ((z - hop, z - hop >= 0), (z + hop, z + hop < Z)):
+            at = jnp.clip(zs, 0, Z - 1)
+
+            @pl.when(there)
+            def _():
+                act_on(at)
+
+    def shared_hop(hop):
+        line(shb, by_f, sh_s, sh_r, hop)
+        line(sdb, by_f, sd_s, sd_r, hop)
+        if hop:
+            come(hop, shared_y)
+        else:
+            shared_y(z)
+
+    pl.semaphore_wait(greet, E + Pn - 2)
+    shared_hop(0)
     wide = max(16, E)
-    gcol[...] = jnp.broadcast_to(gain[...], (128, S.Dr)).T
-    lanes = lax.broadcasted_iota(jnp.int32, (T, 128), 1)
-    routes = route[...].astype(F32)
-    named0, named1 = routes[:, 0:1], routes[:, 1:2]
-    by_row = jnp.where(lanes == 0, named0, named1).T
-    r0, r1 = by_row[0:1, :], by_row[1:2, :]
+    r0, r1 = route[0:1, :].astype(F32), route[1:2, :].astype(F32)
     names = lax.broadcasted_iota(jnp.int32, (wide, T), 0).astype(F32)
     hit0, hit1 = r0 == names, r1 == names
     chosen = (hit0 | hit1).astype(F32).astype(BF16)
@@ -131,6 +187,7 @@
     info[z, 1:2, :] = r1
     info[z, 2:3, :] = s0
     info[z, 3:4, :] = s1
+    info[z, 4:6, :] = weight[...]
 
     tok_load.wait()
     tile = min(64, T)
@@ -144,48 +201,6 @@
 
     loop(T // tile, normalise)
 
-    for copy in sh_loads:
-        copy.wait()
-    shb[f, :, 0:Sc] = (gcol[:, 0:1] * wbuf[1, 0]).astype(BF16)
-    shb[f, :, Sc:] = (gcol[:, 0:1] * wbuf[1, 1]).astype(BF16)
-    sdb[f] = dbuf[1].astype(BF16)
-
-    by_z = lambda zs: zs
-    by_f = lambda zs: zs * Y + y
-
-    pl.semaphore_wait(greet, E + Pn - 2)
-
-    def lanes_of(slot_of, hop, within):
-        low, high = (1, Z - 1) if within else (0, Z)
-        for d in range(2):
-            zs = z - hop if d == 0 else z + hop
-            there = (zs >= 0) if d == 0 else (zs < Z)
-            if within and hop:
-                there &= inner
-            onward = (z + 1 < high) if d == 0 else (z > low)
-            yield d, there, onward, slot_of(jnp.clip(zs, 0, Z - 1)), f + Y if d == 0 else f - Y
-
-    def line(buf, slot_of, ssem, rsem, hop, within=False):
-        for d, there, onward, slot, nxt in lanes_of(slot_of, hop, within):
-
-            @pl.when(there)
-            def _():
-                if hop:
-                    arrived(buf.at[slot], rsem.at[slot])
-
-                @pl.when(onward)
-                def _():
-                    rcopy(
-                        buf.at[slot], buf.at[slot], ssem.at[d, hop], rsem.at[slot], (nxt, t)
-                    ).start()
-
-    def line_sent(buf, slot_of, ssem, hop, within=False):
-        for d, there, onward, slot, nxt in lanes_of(slot_of, hop, within):
-
-            @pl.when(there & onward)
-            def _():
-                sent(buf.at[slot], ssem.at[d, hop])
-
     def tell(act_on):
         for i in range(1, Z):
             zo = (z + i) % Z
@@ -223,13 +238,6 @@
             load_d(k + 1, 1 - slot).start()
 
         dst[k] = dbuf[slot].astype(BF16)
-
-    def shared_y(zs):
-        s = by_f(zs)
-        for j in range(1, Y):
-            to = (z * Y + (y + j) % Y, t)
-            rcopy(shb.at[s], shb.at[s], shy_s.at[j - 1], sh_r.at[s], to).start()
-            rcopy(sdb.at[s], sdb.at[s], sdy_s.at[j - 1], sd_r.at[s], to).start()
 
     def x_out(s):
         for i in range(1, C):
@@ -296,14 +304,6 @@
         e = peer(k)
         rcopy(dst.at[k], dnb.at[f], dn_s.at[k], dn_r.at[f], (e, t)).start()
 
-    def come(hop, act_on):
-        for zs, there in ((z - hop, z - hop >= 0), (z + hop, z + hop < Z)):
-            at = jnp.clip(zs, 0, Z - 1)
-
-            @pl.when(there)
-            def _():
-                act_on(at)
-
     def pick_come(at):
         arrived(info.at[at], info_r.at[at])
         pick(at)
@@ -314,31 +314,24 @@
         @pl.when(inner)
         def _():
             come(hop, pick_come)
-
-    def shared_hop(hop):
-        line(shb, by_f, sh_s, sh_r, hop)
-        line(sdb, by_f, sd_s, sd_r, hop)
-        if hop:
-            come(hop, shared_y)
-        else:
-            shared_y(z)
 
     pick(z)
     loop(E, convert_gu)
     loop(E, convert_dn)
     gub[f] = gst[E - 1]
     dnb[f] = dst[E - 1]
+    for hop in range(1, Z - 1):
+        tok_hop(hop)
+        shared_hop(hop)
+        line_sent(tok, by_z, tok_s, hop - 1, True)
+        line_sent(shb, by_f, sh_s, hop - 1)
+        line_sent(sdb, by_f, sd_s, hop - 1)
+    if Z == 2:
+        line_sent(tok, by_z, tok_s, 0, True)
+        line_sent(shb, by_f, sh_s, 0)
+        line_sent(sdb, by_f, sd_s, 0)
     if Z > 2:
-        tok_hop(1)
-    line_sent(tok, by_z, tok_s, 0, True)
-    if Z > 2:
-        line_sent(tok, by_z, tok_s, 1, True)
-    shared_hop(0)
-    for hop in range(2, Z - 1):
-        tok_hop(hop)
-    shared_hop(1)
-    line_sent(shb, by_f, sh_s, 0)
-    line_sent(sdb, by_f, sd_s, 0)
+        line_sent(tok, by_z, tok_s, Z - 2, True)
     loop(half // 2, send_gu)
     loop(E - 1, send_gu, half)
 
@@ -356,10 +349,9 @@
                     arrived(rows.at[t, s], rows_r.at[t, s])
                     x_out(s)
 
-    for hop in range(2, Z - 1):
-        shared_hop(hop)
     loop(half // 2, lambda k: sent(gst.at[k], gu_s.at[k]))
     loop(half, send_gu, half // 2)
+    loop(E - 1, send_dn, half)
     for i in range(1, C):
         to_t = (x + i) % C * cores + c
 
@@ -371,9 +363,6 @@
             ).start()
 
         loop(E, forward)
-    loop(half, lambda k: sent(gst.at[k], gu_s.at[k]), half // 2)
-    loop(E - 1, send_dn)
-
     def put(src, dst_ref, i):
         copy = pltpu.make_async_copy(src, dst_ref, out_sem.at[i])
         copy.start()
@@ -398,6 +387,10 @@
             at = pl.ds(pl.multiple_of(tt * Dc, Dc), Dc)
             arrived(out.at[:, :, at], rsem.at[tt])
 
+    if Z > 2:
+        shared_hop(Z - 1)
+    loop(half, lambda k: sent(gst.at[k], gu_s.at[k]), half // 2)
+
     def act(v, width):
         gate, up = v[:, :width], v[:, width:]
         return (gate / (1.0 + jnp.exp(-gate)) * up).astype(BF16)
@@ -413,6 +406,9 @@
             total = term if total is None else total + term
         shid[t, at, :] = act(total, Sc)
 
+    def inner_of(s):
+        return (s // Y > 0) & (s // Y < Z - 1)
+
     def rows_waits():
         part = x * cores + 1 - c
         arrived(rows.at[part], part_r.at[0])
@@ -422,17 +418,25 @@
     rows_waits()
 
     def wait_gu(k):
-        s = source(k)
+        s = peer(k)
         arrived(gub.at[s], gu_r.at[s])
 
     loop(E - 1, wait_gu)
+    loop(half, send_dn)
     puts.append(put(gub.at[:, :, pl.ds(0, Hc)], eg, 4))
     puts.append(put(gub.at[:, :, pl.ds(Hc, Hc)], eu, 5))
     M, g, groups = S.M, S.g, S.groups
     own = f // g
 
+    low = f < half
+    side = groups // 2
+    mid_z = jnp.where(low, Z // 2 - 1, Z // 2)
+    over_z = jnp.where(low, Z // 2, Z // 2 - 1)
+
     def group_at(k):
-        return ring(k, groups, own) if groups > 1 else 0
+        far = jnp.where(low, groups - 1 - k, k)
+        near = own // side * side + (own + 1 + k - side) % side
+        return jnp.where(k < side, far, near)
 
     def hidden_in(k):
         q0 = group_at(k)
@@ -444,13 +448,23 @@
             total = term if total is None else total + term
         hid[t, span] = act(total, Hc).reshape(g, cap, Hc)
 
+    partner = x * cores + 1 - c
+
+    def pass_hidden(i, tt, k, to):
+        span = pl.ds(group_at(k) * g, g)
+        rcopy(hid.at[tt, span], hid.at[tt, span], hid_s.at[i], hid_r.at[tt, k], (f, to)).start()
+
     def send_hidden(k):
+        for i in range(1, C):
+            pass_hidden(i, t, k, (x + i) % C * cores + c)
+        pass_hidden(0, t, k, partner)
+
+    def forward_hidden(k):
         span = pl.ds(group_at(k) * g, g)
-        for j in range(1, Pn):
-            tt = (t + j) % Pn
-            rcopy(
-                hid.at[t, span], hid.at[t, span], hid_s.at[j - 1], hid_r.at[t, k], (f, tt)
-            ).start()
+        for i in range(1, C):
+            tt = (x + i) % C * cores + c
+            arrived(hid.at[tt, span], hid_r.at[tt, k])
+            pass_hidden(C - 1 + i, tt, k, partner)
 
     def hidden_step(k):
         hidden_in(k)
@@ -462,27 +476,44 @@
     loop(groups, hidden_step)
 
     def wait_dn(k):
-        s = source(k)
+        s = peer(k)
         arrived(dnb.at[s], dn_r.at[s])
 
     send_hidden(groups - 1)
-    if Z > 2:
-        shared_hop(Z - 1)
+    for j in range(1, Y):
+        for zs in range(Z):
+            s = zs * Y + (y + j) % Y
+            arrived(shb.at[s], sh_r.at[s])
+            arrived(sdb.at[s], sd_r.at[s])
+
+    puts += [put(shb.at[:, :, pl.ds(0, Sc)], sg, 1), put(shb.at[:, :, pl.ds(Sc, Sc)], su, 2)]
+    loop(T // mt, shared_in)
+
+    for k in range(1, Pn):
+        rcopy(shid.at[t], shid.at[t], shid_s.at[k - 1], shid_r.at[t], (f, (t + k) % Pn)).start()
+    puts.append(spread(sdb, sd, sdo_s, sdo_r, 3))
+    loop(groups, forward_hidden)
     loop(E - 1, wait_dn)
-    puts.append(spread(dnb, ed, edo_s, edo_r, 6))
 
     def send_back(k):
         for i in range(g):
             s = group_at(k) * g + i
-
-            @pl.when(s != f)
+            over = (s // Y == over_z) & inner_of(s)
+            to = mid_z * Y + s % Y
+
+            @pl.when(over & (to != f))
+            def _():
+                rcopy(res.at[s], cmb.at[f % half], ret_s.at[s], cmb_r.at[f % half], (to, t)).start()
+
+            @pl.when(jnp.logical_not(over) & (s != f))
             def _():
                 rcopy(res.at[s], ret.at[f], ret_s.at[s], ret_r.at[f], (s, t)).start()
 
     def back_step(k):
         span = pl.ds(group_at(k) * g, g)
-        for j in range(1, Pn):
-            tt = (t + j) % Pn
+
+        for i in range(C):
+            tt = (x + i) % C * cores + 1 - c
             arrived(hid.at[tt, span], hid_r.at[tt, k])
 
         def part(n):
@@ -500,17 +531,34 @@
     loop(groups, back_step)
     ret[f] = res[f]
 
-    for j in range(1, Y):
-        for zs in range(Z):
-            s = zs * Y + (y + j) % Y
-            arrived(shb.at[s], sh_r.at[s])
-            arrived(sdb.at[s], sd_r.at[s])
-
-    puts += [put(shb.at[:, :, pl.ds(0, Sc)], sg, 1), put(shb.at[:, :, pl.ds(Sc, Sc)], su, 2)]
-    loop(T // mt, shared_in)
-
-    for k in range(1, Pn):
-        rcopy(shid.at[t], shid.at[t], shid_s.at[k - 1], shid_r.at[t], (f, (t + k) % Pn)).start()
+    def weigh(zs, base, many):
+        spot = (lax.broadcasted_iota(jnp.int32, (many, T), 0) + base).astype(F32)
+        at0 = info[zs, 0:1, :] * cap + info[zs, 2:3, :]
+        at1 = info[zs, 1:2, :] * cap + info[zs, 3:4, :]
+        share = jnp.where(at0 == spot, info[zs, 4:5, :], 0.0)
+        share += jnp.where(at1 == spot, info[zs, 5:6, :], 0.0)
+        return share.T.astype(BF16)
+
+    puts.append(spread(dnb, ed, edo_s, edo_r, 6))
+    @pl.when(inner)
+    def _():
+        to = over_z * Y + y
+        cmb[f % half] = res[to]
+        for i in range(1, half):
+            e = (f + i) % half
+            arrived(cmb.at[e], cmb_r.at[e])
+        many = half * cap
+        shares = weigh(over_z, f // half * many, many)
+
+        def part(n):
+            at = pl.ds(pl.multiple_of(n * nt, nt), nt)
+            block = cmb[:, :, at].reshape(many, nt)
+            tok[0, :, at] = jnp.dot(shares, block, preferred_element_type=F32).astype(BF16)
+
+        loop(Dc // nt, part)
+        rcopy(tok.at[0], farin, far_s.at[0], far_r.at[0], (to, t)).start()
+
+
     for k in range(1, Pn):
         arrived(shid.at[(t + k) % Pn], shid_r.at[(t + k) % Pn])
 
@@ -525,25 +573,9 @@
 
     loop(Dc // nt, shared_out)
 
-    puts.append(spread(sdb, sd, sdo_s, sdo_r, 3))
-
-    routes = route[...].astype(F32)
-    named0, named1 = routes[:, 0:1], routes[:, 1:2]
-    name_cols = lax.broadcasted_iota(jnp.int32, (T, 128), 1).astype(F32)
-    is0, is1 = named0 == name_cols, named1 == name_cols
-    chosen_cols = (is0 | is1).astype(F32)
-    after = lax.broadcasted_iota(jnp.int32, (T, T), 0) > lax.broadcasted_iota(
-        jnp.int32, (T, T), 1
-    )
-    count_cols = jnp.dot(
-        after.astype(F32).astype(BF16), chosen_cols.astype(BF16), preferred_element_type=F32
-    )
-    target0 = named0 * cap + jnp.sum(jnp.where(is0, count_cols, 0.0), axis=1, keepdims=True)
-    target1 = named1 * cap + jnp.sum(jnp.where(is1, count_cols, 0.0), axis=1, keepdims=True)
-    w0, w1 = weight[:, 0:1], weight[:, 1:2]
-
-    def combine(i):
-        q0 = group_at(groups - 1 - i)
+
+    def combine(k):
+        q0 = group_at(groups - 1 - k)
         for j in range(g):
             s = q0 * g + j
 
@@ -551,27 +583,32 @@
             def _():
                 arrived(ret.at[s], ret_r.at[s])
 
-        spot = (lax.broadcasted_iota(jnp.int32, (T, M), 1) + q0 * M).astype(F32)
-        weigh = jnp.where(target0 == spot, w0, 0.0) + jnp.where(target1 == spot, w1, 0.0)
-        weigh = weigh.astype(BF16)
+        shares = weigh(z, q0 * M, M)
 
         def part(n):
             at = pl.ds(pl.multiple_of(n * nt, nt), nt)
             block = ret[pl.ds(q0 * g, g), :, at].reshape(M, nt)
-            total = acc[:, at] + jnp.dot(weigh, block, preferred_element_type=F32)
-            acc[:, at] = total
+            acc[:, at] += jnp.dot(shares, block, preferred_element_type=F32)
 
         loop(Dc // nt, part)
 
-    loop(groups, combine)
+    loop(side, combine)
+
+    @pl.when(jnp.logical_not(inner))
+    def _():
+        loop(groups, combine, side)
+
+    @pl.when(inner)
+    def _():
+        arrived(farin, far_r.at[0])
+        acc[...] += farin[...].astype(F32)
+
     outb[...] = acc[...].astype(BF16)
     puts.append(put(outb, mixed, 7))
 
-    for hop in range(1, Z - 1):
-        if hop > 1:
-            line_sent(tok, by_z, tok_s, hop, True)
-        line_sent(shb, by_f, sh_s, hop)
-        line_sent(sdb, by_f, sd_s, hop)
+    if Z > 2:
+        line_sent(shb, by_f, sh_s, Z - 2)
+        line_sent(sdb, by_f, sd_s, Z - 2)
     tell(lambda i, zo: sent(info.at[z], info_s.at[i]))
     for j in range(1, Y):
         sent(shb.at[pl.ds(0, Z)], shy_s.at[j - 1])
@@ -601,8 +638,15 @@
         sent(hid.at[t], hid_s.at[k - 1])
 
     def drain_ret(k):
-        s = source(k)
-        sent(res.at[s], ret_s.at[s])
+        s = peer(k)
+
+        @pl.when(jnp.logical_not(inner & (s == over_z * Y + y)))
+        def _():
+            sent(res.at[s], ret_s.at[s])
+
+    @pl.when(inner)
+    def _():
+        sent(tok.at[0], far_s.at[0])
 
     loop(E - 1, drain_ret)
     spread_wait(sdb, sd, sdo_s, sdo_r)
@@ -668,6 +712,8 @@
         pltpu.VMEM((Pn, E, cap, Hc), BF16),
         pltpu.VMEM((E, cap, Dc), BF16),
         pltpu.VMEM((E, cap, Dc), BF16),
+        pltpu.VMEM((E // 2, cap, Dc), BF16),
+        pltpu.VMEM((T, Dc), BF16),
         pltpu.VMEM((T, Dc), F32),
         pltpu.VMEM((Pn, T, Sc), BF16),
         pltpu.VMEM((T, Dc), BF16),
@@ -683,6 +729,7 @@
         dma((Pn,)), dma((Pn, S.groups)), dma((Pn,)), dma((Pn,)),
         dma((Pn,)), dma((Pn,)), dma((Pn,)), dma((Pn,)),
         dma((E,)), dma((E,)),
+        dma((E // 2,)), dma((1,)), dma((1,)),
     ]
     shape = lambda *dims: jax.ShapeDtypeStruct(dims, BF16)
     flops = 2 * T * D * 2 * Sc + 2 * E * cap * D * 2 * Hc + 4 * E * cap * D * Hc
@@ -701,7 +748,7 @@
         cost_estimate=pl.CostEstimate(flops=flops, bytes_accessed=1 << 26, transcendentals=0),
     )(
         tokens, gate_train, up_train, down_train, shared_gate_train, shared_up_train,
-        shared_down_train, norm_gain[None, :], route_expert, route_weight,
+        shared_down_train, norm_gain[None, :], route_expert.T, route_weight.T,
     )
     parts = 2
     in_hbm = pl.BlockSpec(memory_space=pl.ANY)

time: 326 us -> 294 us (0.902)
  the two profiles are of different devices: /device:TPU:1 before, /device:TPU:20 now
where the time goes in v2:
time: 294 us; the launch traced here: 292 us
  Pallas kernels  292 us (99%)
    pallas_call x1, Pallas kernels, on_device(): pl.pallas_call(functools.partial(kernel, S), out_shape=[shape(E, Dr, Hc),...  282 us
    pallas_call x1, Pallas kernels, on_device(): pl.pallas_call(functools.partial(handed, len(outs), parts), out_shape=[ja...  9.72 us

profile of v2, /device:TPU:20, one launch (start us, length us, event | category | flops | bytes accessed | tf_op | source)
XLA Modules:
  0.0 292.4 jit_solution(9098837130674725902)
XLA Ops:
  0.6 281.8 %shard_map.153 = (bf16[8,512,256]{2,1,0:T(8,128)(2,1)}, bf16[8,512,256]{2,1,0:T(8,128)(2,1)}, bf16[2,128,4096]{2,1,0:T(8,128)(2,1)}, bf16[8,512,256]{2,1,0:T(8,1...) custom-call(bf16[512,4096]{1,0:T(8,128)(2,1)} %tokens.1, ...), custom_call_target="tpu_custom_call" | custom-call | flops 15032385536 | bytes 67108864 | tf_op jit(solution)/shard_map/pallas_call | solution.py:736
  282.5 9.7 %shard_map.154 = (bf16[8,512,256]{2,1,0:T(8,128)(2,1)}, bf16[8,512,256]{2,1,0:T(8,128)(2,1)}, bf16[2,128,4096]{2,1,0:T(8,128)(2,1)}, bf16[8,512,256]{2,1,0:T(8,1...) custom-call(bf16[8,512,256]{2,1,0:T(8,128)(2,1)} %get-tuple-element.21.refs_0_, ...), custom_call_target="tpu_custom_call" | custom-call | tf_op jit(solution)/shard_map/pallas_call | solution.py:755

commit v3 on v2

--- a/solution.py
+++ b/solution.py
@@ -1,4 +1,5 @@
 import functools
+import math
 
 import jax
 import jax.numpy as jnp
@@ -35,13 +36,14 @@
         self.groups = experts // self.g
         self.M = self.g * self.cap
         self.nt = min(256, self.Dc)
+        assert self.groups <= self.Z and self.M <= self.T
 
 
 def kernel(
     S,
     tokens, gate_t, up_t, down_t, sgate_t, sup_t, sdown_t, gain, route, weight,
-    eg, eu, ed, sg, su, sd, mixed,
-    nrm, tok, info, shb, sdb, gst, gub, dst, dnb, rows, yst, est, hid, res, ret, cmb, farin, acc, shid, outb,
+    gub, shb, outb, ed, sd,
+    nrm, tok, info, sdb, gst, dst, dnb, rows, yst, est, hid, ret, cmb, farin, acc, shid,
     wbuf, dbuf, gcol,
     ld_sem, tk_ld, out_sem,
     tok_s, tok_r, info_s, info_r, sh_s, sh_r, shy_s, sd_s, sd_r, sdy_s,
@@ -423,8 +425,6 @@
 
     loop(E - 1, wait_gu)
     loop(half, send_dn)
-    puts.append(put(gub.at[:, :, pl.ds(0, Hc)], eg, 4))
-    puts.append(put(gub.at[:, :, pl.ds(Hc, Hc)], eu, 5))
     M, g, groups = S.M, S.g, S.groups
     own = f // g
 
@@ -434,7 +434,8 @@
     over_z = jnp.where(low, Z // 2, Z // 2 - 1)
 
     def group_at(k):
-        far = jnp.where(low, groups - 1 - k, k)
+        at = jnp.where(inner, k, side - 1 - k)
+        far = jnp.where(low, groups - 1 - at, at)
         near = own // side * side + (own + 1 + k - side) % side
         return jnp.where(k < side, far, near)
 
@@ -486,7 +487,6 @@
             arrived(shb.at[s], sh_r.at[s])
             arrived(sdb.at[s], sd_r.at[s])
 
-    puts += [put(shb.at[:, :, pl.ds(0, Sc)], sg, 1), put(shb.at[:, :, pl.ds(Sc, Sc)], su, 2)]
     loop(T // mt, shared_in)
 
     for k in range(1, Pn):
@@ -495,6 +495,9 @@
     loop(groups, forward_hidden)
     loop(E - 1, wait_dn)
 
+    def res_at(s):
+        return tok.at[s // g, pl.ds(pl.multiple_of(s % g * cap, cap), cap)]
+
     def send_back(k):
         for i in range(g):
             s = group_at(k) * g + i
@@ -503,11 +506,11 @@
 
             @pl.when(over & (to != f))
             def _():
-                rcopy(res.at[s], cmb.at[f % half], ret_s.at[s], cmb_r.at[f % half], (to, t)).start()
+                rcopy(res_at(s), cmb.at[f % half], ret_s.at[s], cmb_r.at[f % half], (to, t)).start()
 
             @pl.when(jnp.logical_not(over) & (s != f))
             def _():
-                rcopy(res.at[s], ret.at[f], ret_s.at[s], ret_r.at[f], (s, t)).start()
+                rcopy(res_at(s), ret.at[f], ret_s.at[s], ret_r.at[f], (s, t)).start()
 
     def back_step(k):
         span = pl.ds(group_at(k) * g, g)
@@ -523,13 +526,13 @@
                 w = dnb[q * per : (q + 1) * per, :, at].reshape(Hc, nt)
                 term = jnp.dot(hid[q, span].reshape(M, Hc), w, preferred_element_type=F32)
                 total = term if total is None else total + term
-            res[span, :, at] = total.astype(BF16).reshape(g, cap, nt)
+            tok[group_at(k), 0:M, at] = total.astype(BF16)
 
         loop(Dc // nt, part)
         send_back(k)
 
     loop(groups, back_step)
-    ret[f] = res[f]
+    ret[f] = res_at(f)[...]
 
     def weigh(zs, base, many):
         spot = (lax.broadcasted_iota(jnp.int32, (many, T), 0) + base).astype(F32)
@@ -543,7 +546,7 @@
     @pl.when(inner)
     def _():
         to = over_z * Y + y
-        cmb[f % half] = res[to]
+        cmb[f % half] = res_at(to)[...]
         for i in range(1, half):
             e = (f + i) % half
             arrived(cmb.at[e], cmb_r.at[e])
@@ -553,10 +556,10 @@
         def part(n):
             at = pl.ds(pl.multiple_of(n * nt, nt), nt)
             block = cmb[:, :, at].reshape(many, nt)
-            tok[0, :, at] = jnp.dot(shares, block, preferred_element_type=F32).astype(BF16)
+            nrm[:, at] = jnp.dot(shares, block, preferred_element_type=F32).astype(BF16)
 
         loop(Dc // nt, part)
-        rcopy(tok.at[0], farin, far_s.at[0], far_r.at[0], (to, t)).start()
+        rcopy(nrm.at[:, pl.ds(0, Dc)], farin, far_s.at[0], far_r.at[0], (to, t)).start()
 
 
     for k in range(1, Pn):
@@ -604,7 +607,6 @@
         acc[...] += farin[...].astype(F32)
 
     outb[...] = acc[...].astype(BF16)
-    puts.append(put(outb, mixed, 7))
 
     if Z > 2:
         line_sent(shb, by_f, sh_s, Z - 2)
@@ -642,11 +644,11 @@
 
         @pl.when(jnp.logical_not(inner & (s == over_z * Y + y)))
         def _():
-            sent(res.at[s], ret_s.at[s])
+            sent(res_at(s), ret_s.at[s])
 
     @pl.when(inner)
     def _():
-        sent(tok.at[0], far_s.at[0])
+        sent(nrm.at[:, pl.ds(0, Dc)], far_s.at[0])
 
     loop(E - 1, drain_ret)
     spread_wait(sdb, sd, sdo_s, sdo_r)
@@ -655,28 +657,28 @@
         copy.wait()
 
 
-def handed(count, parts, *refs):
-    ins, outs, held = refs[:count], refs[count : 2 * count], refs[2 * count : 3 * count]
-    in_sem, out_sem = refs[3 * count :]
-
-    def piece(i, j, ref):
-        rows = ref.shape[0] // parts
-        return ref.at[pl.ds(j * rows, rows)]
-
-    def taken(i, j):
-        return pltpu.make_async_copy(piece(i, j, ins[i]), piece(i, j, held[i]), in_sem.at[i, j])
-
-    def given(i, j):
-        return pltpu.make_async_copy(piece(i, j, held[i]), piece(i, j, outs[i]), out_sem.at[i, j])
-
-    every = [(i, j) for i in range(count) for j in range(parts)]
-    for at in every:
-        taken(*at).start()
-    for at in every:
-        taken(*at).wait()
-        given(*at).start()
-    for at in every:
-        given(*at).wait()
+def handed(S, gub, shb, outb, ed, sd, eg, eu, sg, su, mixed, ed_out, sd_out, held, kept, sem):
+    Hc, Sc = S.Hc, S.Sc
+    loads = [
+        pltpu.make_async_copy(ed, held, sem.at[0]),
+        pltpu.make_async_copy(sd, kept, sem.at[1]),
+    ]
+    stores = [
+        pltpu.make_async_copy(gub.at[:, :, pl.ds(0, Hc)], eg, sem.at[2]),
+        pltpu.make_async_copy(gub.at[:, :, pl.ds(Hc, Hc)], eu, sem.at[3]),
+        pltpu.make_async_copy(shb.at[:, :, pl.ds(0, Sc)], sg, sem.at[4]),
+        pltpu.make_async_copy(shb.at[:, :, pl.ds(Sc, Sc)], su, sem.at[5]),
+        pltpu.make_async_copy(outb, mixed, sem.at[6]),
+    ]
+    for copy in loads + stores:
+        copy.start()
+    for i, (load, buf, out) in enumerate(zip(loads, (held, kept), (ed_out, sd_out))):
+        load.wait()
+        store = pltpu.make_async_copy(buf, out, sem.at[7 + i])
+        store.start()
+        stores.append(store)
+    for copy in stores:
+        copy.wait()
 
 
 def on_device(
@@ -700,9 +702,7 @@
         pltpu.VMEM((T, D), BF16),
         pltpu.VMEM((Z, T, Dc), BF16),
         pltpu.VMEM((Z, 8, T), F32),
-        pltpu.VMEM((E, Dr, 2 * Sc), BF16),
         pltpu.VMEM((E, Sr, Dc), BF16),
-        pltpu.VMEM((E, Dr, 2 * Hc), BF16),
         pltpu.VMEM((E, Dr, 2 * Hc), BF16),
         pltpu.VMEM((E, Hr, Dc), BF16),
         pltpu.VMEM((E, Hr, Dc), BF16),
@@ -711,12 +711,10 @@
         pltpu.VMEM((Z, Y, cap, Dc), BF16),
         pltpu.VMEM((Pn, E, cap, Hc), BF16),
         pltpu.VMEM((E, cap, Dc), BF16),
-        pltpu.VMEM((E, cap, Dc), BF16),
         pltpu.VMEM((E // 2, cap, Dc), BF16),
         pltpu.VMEM((T, Dc), BF16),
         pltpu.VMEM((T, Dc), F32),
         pltpu.VMEM((Pn, T, Sc), BF16),
-        pltpu.VMEM((T, Dc), BF16),
         pltpu.VMEM((2, 2, Dr, Hc), F32),
         pltpu.VMEM((2, Hr, Dc), F32),
         pltpu.VMEM((Dr, 128), F32),
@@ -733,34 +731,40 @@
     ]
     shape = lambda *dims: jax.ShapeDtypeStruct(dims, BF16)
     flops = 2 * T * D * 2 * Sc + 2 * E * cap * D * 2 * Hc + 4 * E * cap * D * Hc
+    vmem = pltpu.MemorySpace.VMEM
+    handed_on = [(E, Dr, 2 * Hc), (E, Dr, 2 * Sc), (T, Dc)]
+    limit = 66781184 - 2 * sum(math.prod(dims) for dims in handed_on)
     outs = pl.pallas_call(
         functools.partial(kernel, S),
-        out_shape=[
-            shape(E, Dr, Hc), shape(E, Dr, Hc), shape(per, Hr, D),
-            shape(E, Dr, Sc), shape(E, Dr, Sc), shape(per, Sr, D), shape(T, Dc),
-        ],
+        out_shape=[vmem(dims, BF16) for dims in handed_on]
+        + [shape(per, Hr, D), shape(per, Sr, D)],
         in_specs=[anywhere] * 7 + [inside] * 3,
-        out_specs=[anywhere] * 7,
+        out_specs=[inside] * 3 + [anywhere] * 2,
         scratch_shapes=scratch,
         compiler_params=pltpu.CompilerParams(
-            collective_id=0, has_side_effects=True, vmem_limit_bytes=67043328
+            collective_id=0, has_side_effects=True, vmem_limit_bytes=limit
         ),
         cost_estimate=pl.CostEstimate(flops=flops, bytes_accessed=1 << 26, transcendentals=0),
     )(
         tokens, gate_train, up_train, down_train, shared_gate_train, shared_up_train,
         shared_down_train, norm_gain[None, :], route_expert.T, route_weight.T,
     )
-    parts = 2
-    in_hbm = pl.BlockSpec(memory_space=pl.ANY)
-    eg, eu, ed, sg, su, sd, mixed = pl.pallas_call(
-        functools.partial(handed, len(outs), parts),
-        out_shape=[jax.ShapeDtypeStruct(o.shape, o.dtype) for o in outs],
-        in_specs=[in_hbm] * len(outs),
-        out_specs=[in_hbm] * len(outs),
-        scratch_shapes=[pltpu.VMEM(o.shape, o.dtype) for o in outs]
-        + [dma((len(outs), parts))] * 2,
-        compiler_params=pltpu.CompilerParams(vmem_limit_bytes=62 << 20),
-    )(*outs)
+    eg, eu, sg, su, mixed, ed, sd = pl.pallas_call(
+        functools.partial(handed, S),
+        out_shape=[
+            shape(E, Dr, Hc), shape(E, Dr, Hc), shape(E, Dr, Sc), shape(E, Dr, Sc),
+            shape(T, Dc), shape(per, Hr, D), shape(per, Sr, D),
+        ],
+        in_specs=[inside] * 3 + [anywhere] * 2,
+        out_specs=[anywhere] * 7,
+        scratch_shapes=[
+            pltpu.VMEM((per, Hr, D), BF16), pltpu.VMEM((per, Sr, D), BF16), dma((9,))
+        ],
+        compiler_params=pltpu.CompilerParams(vmem_limit_bytes=1 << 25),
+    )(
+        *[pltpu.with_memory_space_constraint(o, vmem) for o in outs[:3]],
+        *[pltpu.with_memory_space_constraint(o, pltpu.MemorySpace.HBM) for o in outs[3:]],
+    )
     return (
         eg.reshape(1, D, Hc), eu.reshape(1, D, Hc), ed.reshape(1, per * Hr, D),
         sg.reshape(D, Sc), su.reshape(D, Sc), sd.reshape(per * Sr, D), mixed,

time: 294 us -> 291 us (0.990)
  no operation moved by 1% of the time
where the time goes in v3:
time: 291 us; the launch traced here: 290 us
  Pallas kernels  290 us (100%)
    pallas_call x1, Pallas kernels, on_device(): pl.pallas_call(functools.partial(kernel, S), out_shape=[vmem(dims, BF16)...  283 us
    pallas_call x1, Pallas kernels, on_device(): pl.pallas_call(functools.partial(handed, S), out_shape=[shape(E, Dr, Hc),...  6.62 us

profile of v3, /device:TPU:20, one launch (start us, length us, event | category | flops | bytes accessed | tf_op | source)
XLA Modules:
  0.0 290.4 jit_solution(16846946012067142494)
XLA Ops:
  0.6 282.9 %shard_map.153 = (bf16[8,512,512]{2,1,0:T(8,128)(2,1)S(1)}, bf16[8,512,512]{2,1,0:T(8,128)(2,1)S(1)}, bf16[512,1024]{1,0:T(8,128)(2,1)S(1)}, bf16[2,128,4096]{2,1,0:T(8,128)(2,1)}, bf16[2,128,4096]{2,1,0:T(8,128)(2,1)}) custom-call(bf16[512,4096]{1,0:T(8,128)(2,1)} %tokens.1, f32[8,512,256]{2,1,0:T(8,128)} %gate_t.1, f32[8,512,256]{2,1,0:T(8,128)} %up_t.1, ...), custom_call_target="tpu_custom_call" | custom-call | flops 15032385536 | bytes 67108864 | tf_op jit(solution)/shard_map/pallas_call | solution.py:737
  283.6 6.6 %shard_map.154 = (bf16[8,512,256]{2,1,0:T(8,128)(2,1)}, bf16[8,512,256]{2,1,0:T(8,128)(2,1)}, bf16[8,512,256]{2,1,0:T(8,128)(2,1)}, bf16[8,512,256]{2,1,0:T(8,12...) custom-call(bf16[8,512,512]{2,1,0:T(8,128)(2,1)S(1)} %get-tuple-element.19.gub, ...), custom_call_target="tpu_custom_call" | custom-call | tf_op jit(solution)/shard_map/pallas_call | solution.py:752

commit v4 on v3

--- a/solution.py
+++ b/solution.py
@@ -44,7 +44,7 @@
     tokens, gate_t, up_t, down_t, sgate_t, sup_t, sdown_t, gain, route, weight,
     gub, shb, outb, ed, sd,
     nrm, tok, info, sdb, gst, dst, dnb, rows, yst, est, hid, ret, cmb, farin, acc, shid,
-    wbuf, dbuf, gcol,
+    dbuf, gcol,
     ld_sem, tk_ld, out_sem,
     tok_s, tok_r, info_s, info_r, sh_s, sh_r, shy_s, sd_s, sd_r, sdy_s,
     gu_s, gu_r, dn_s, dn_r, y_s, e_s, rows_r, x_s, part_s, part_r,
@@ -81,10 +81,14 @@
     def loop(count, body, start=0):
         lax.fori_loop(start, count, lambda i, v: (body(i), v)[1], 0)
 
+    def passing(slot, i):
+        at = pl.multiple_of((slot * 2 + i) * Hc, Hc)
+        return acc.at[pl.ds(0, S.Dr), pl.ds(at, Hc)]
+
     def load_w(k, slot):
         e = peer(k)
         return [
-            pltpu.make_async_copy(w.at[e], wbuf.at[slot, i], ld_sem.at[slot, i])
+            pltpu.make_async_copy(w.at[e], passing(slot, i), ld_sem.at[slot, i])
             for i, w in ((0, gate_t), (1, up_t))
         ]
 
@@ -94,8 +98,8 @@
     tok_load = pltpu.make_async_copy(tokens, nrm, tk_ld.at[0])
     tok_load.start()
     sh_loads = [
-        pltpu.make_async_copy(sgate_t, wbuf.at[1, 0], ld_sem.at[1, 0]),
-        pltpu.make_async_copy(sup_t, wbuf.at[1, 1], ld_sem.at[1, 1]),
+        pltpu.make_async_copy(sgate_t, passing(1, 0), ld_sem.at[1, 0]),
+        pltpu.make_async_copy(sup_t, passing(1, 1), ld_sem.at[1, 1]),
         pltpu.make_async_copy(sdown_t, dbuf.at[1], ld_sem.at[1, 2]),
     ]
     for copy in sh_loads + load_w(0, 0) + [load_d(0, 0)]:
@@ -110,8 +114,8 @@
     gcol[...] = jnp.broadcast_to(gain[...], (128, S.Dr)).T
     for copy in sh_loads:
         copy.wait()
-    shb[f, :, 0:Sc] = (gcol[:, 0:1] * wbuf[1, 0]).astype(BF16)
-    shb[f, :, Sc:] = (gcol[:, 0:1] * wbuf[1, 1]).astype(BF16)
+    shb[f, :, 0:Sc] = (gcol[:, 0:1] * passing(1, 0)[...]).astype(BF16)
+    shb[f, :, Sc:] = (gcol[:, 0:1] * passing(1, 1)[...]).astype(BF16)
     sdb[f] = dbuf[1].astype(BF16)
 
     by_z = lambda zs: zs
@@ -229,7 +233,7 @@
                 copy.start()
 
         for i in range(2):
-            gst[k, :, i * Hc : (i + 1) * Hc] = (gcol[:, 0:1] * wbuf[slot, i]).astype(BF16)
+            gst[k, :, i * Hc : (i + 1) * Hc] = (gcol[:, 0:1] * passing(slot, i)[...]).astype(BF16)
 
     def convert_dn(k):
         slot = k % 2
@@ -365,22 +369,16 @@
             ).start()
 
         loop(E, forward)
-    def put(src, dst_ref, i):
-        copy = pltpu.make_async_copy(src, dst_ref, out_sem.at[i])
-        copy.start()
-        return copy
-
-    puts = []
     own_cols = pl.ds(pl.multiple_of(t * Dc, Dc), Dc)
 
-    def spread(buf, out, ssem, rsem, i):
+    def spread(buf, out, ssem, rsem):
         for k in range(1, Pn):
             tt = (t + k) % Pn
             rcopy(
                 buf.at[pl.ds(tt * per, per)], out.at[:, :, own_cols], ssem.at[k - 1],
                 rsem.at[t], (f, tt),
             ).start()
-        return put(buf.at[pl.ds(t * per, per)], out.at[:, :, own_cols], i)
+        out[:, :, own_cols] = buf[pl.ds(t * per, per)]
 
     def spread_wait(buf, out, ssem, rsem):
         for k in range(1, Pn):
@@ -491,7 +489,7 @@
 
     for k in range(1, Pn):
         rcopy(shid.at[t], shid.at[t], shid_s.at[k - 1], shid_r.at[t], (f, (t + k) % Pn)).start()
-    puts.append(spread(sdb, sd, sdo_s, sdo_r, 3))
+    spread(sdb, sd, sdo_s, sdo_r)
     loop(groups, forward_hidden)
     loop(E - 1, wait_dn)
 
@@ -542,7 +540,7 @@
         share += jnp.where(at1 == spot, info[zs, 5:6, :], 0.0)
         return share.T.astype(BF16)
 
-    puts.append(spread(dnb, ed, edo_s, edo_r, 6))
+    spread(dnb, ed, edo_s, edo_r)
     @pl.when(inner)
     def _():
         to = over_z * Y + y
@@ -579,6 +577,7 @@
 
     def combine(k):
         q0 = group_at(groups - 1 - k)
+        shares = weigh(z, q0 * M, M)
         for j in range(g):
             s = q0 * g + j
 
@@ -586,7 +585,6 @@
             def _():
                 arrived(ret.at[s], ret_r.at[s])
 
-        shares = weigh(z, q0 * M, M)
 
         def part(n):
             at = pl.ds(pl.multiple_of(n * nt, nt), nt)
@@ -594,19 +592,6 @@
             acc[:, at] += jnp.dot(shares, block, preferred_element_type=F32)
 
         loop(Dc // nt, part)
-
-    loop(side, combine)
-
-    @pl.when(jnp.logical_not(inner))
-    def _():
-        loop(groups, combine, side)
-
-    @pl.when(inner)
-    def _():
-        arrived(farin, far_r.at[0])
-        acc[...] += farin[...].astype(F32)
-
-    outb[...] = acc[...].astype(BF16)
 
     if Z > 2:
         line_sent(shb, by_f, sh_s, Z - 2)
@@ -635,6 +620,19 @@
         sent(rows.at[t], part_s.at[i])
     loop(E - 1, lambda k: sent(gst.at[k], gu_s.at[k]), half)
     loop(E - 1, lambda k: sent(dst.at[k], dn_s.at[k]))
+    loop(side, combine)
+
+    @pl.when(jnp.logical_not(inner))
+    def _():
+        loop(groups, combine, side)
+        outb[...] = acc[...].astype(BF16)
+
+    @pl.when(inner)
+    def _():
+        arrived(farin, far_r.at[0])
+        outb[...] = (acc[...] + farin[...].astype(F32)).astype(BF16)
+
+
     for k in range(1, Pn):
         sent(shid.at[t], shid_s.at[k - 1])
         sent(hid.at[t], hid_s.at[k - 1])
@@ -653,30 +651,18 @@
     loop(E - 1, drain_ret)
     spread_wait(sdb, sd, sdo_s, sdo_r)
     spread_wait(dnb, ed, edo_s, edo_r)
-    for copy in puts:
-        copy.wait()
-
-
-def handed(S, gub, shb, outb, ed, sd, eg, eu, sg, su, mixed, ed_out, sd_out, held, kept, sem):
+
+
+def handed(S, gub, shb, outb, ed, sd, eg, eu, sg, su, mixed, ed_out, sd_out, sem):
     Hc, Sc = S.Hc, S.Sc
-    loads = [
-        pltpu.make_async_copy(ed, held, sem.at[0]),
-        pltpu.make_async_copy(sd, kept, sem.at[1]),
+    pairs = [
+        (gub.at[:, :, pl.ds(0, Hc)], eg), (gub.at[:, :, pl.ds(Hc, Hc)], eu),
+        (shb.at[:, :, pl.ds(0, Sc)], sg), (shb.at[:, :, pl.ds(Sc, Sc)], su),
+        (outb, mixed), (ed, ed_out), (sd, sd_out),
     ]
-    stores = [
-        pltpu.make_async_copy(gub.at[:, :, pl.ds(0, Hc)], eg, sem.at[2]),
-        pltpu.make_async_copy(gub.at[:, :, pl.ds(Hc, Hc)], eu, sem.at[3]),
-        pltpu.make_async_copy(shb.at[:, :, pl.ds(0, Sc)], sg, sem.at[4]),
-        pltpu.make_async_copy(shb.at[:, :, pl.ds(Sc, Sc)], su, sem.at[5]),
-        pltpu.make_async_copy(outb, mixed, sem.at[6]),
-    ]
-    for copy in loads + stores:
+    stores = [pltpu.make_async_copy(a, b, sem.at[i]) for i, (a, b) in enumerate(pairs)]
+    for copy in stores:
         copy.start()
-    for i, (load, buf, out) in enumerate(zip(loads, (held, kept), (ed_out, sd_out))):
-        load.wait()
-        store = pltpu.make_async_copy(buf, out, sem.at[7 + i])
-        store.start()
-        stores.append(store)
     for copy in stores:
         copy.wait()
 
@@ -715,7 +701,6 @@
         pltpu.VMEM((T, Dc), BF16),
         pltpu.VMEM((T, Dc), F32),
         pltpu.VMEM((Pn, T, Sc), BF16),
-        pltpu.VMEM((2, 2, Dr, Hc), F32),
         pltpu.VMEM((2, Hr, Dc), F32),
         pltpu.VMEM((Dr, 128), F32),
         dma((2, 3)), dma((1,)), dma((8,)),
@@ -732,14 +717,15 @@
     shape = lambda *dims: jax.ShapeDtypeStruct(dims, BF16)
     flops = 2 * T * D * 2 * Sc + 2 * E * cap * D * 2 * Hc + 4 * E * cap * D * Hc
     vmem = pltpu.MemorySpace.VMEM
-    handed_on = [(E, Dr, 2 * Hc), (E, Dr, 2 * Sc), (T, Dc)]
+    handed_on = [
+        (E, Dr, 2 * Hc), (E, Dr, 2 * Sc), (T, Dc), (per, Hr, D), (per, Sr, D)
+    ]
     limit = 66781184 - 2 * sum(math.prod(dims) for dims in handed_on)
     outs = pl.pallas_call(
         functools.partial(kernel, S),
-        out_shape=[vmem(dims, BF16) for dims in handed_on]
-        + [shape(per, Hr, D), shape(per, Sr, D)],
+        out_shape=[vmem(dims, BF16) for dims in handed_on],
         in_specs=[anywhere] * 7 + [inside] * 3,
-        out_specs=[inside] * 3 + [anywhere] * 2,
+        out_specs=[inside] * 5,
         scratch_shapes=scratch,
         compiler_params=pltpu.CompilerParams(
             collective_id=0, has_side_effects=True, vmem_limit_bytes=limit
@@ -755,15 +741,12 @@
             shape(E, Dr, Hc), shape(E, Dr, Hc), shape(E, Dr, Sc), shape(E, Dr, Sc),
             shape(T, Dc), shape(per, Hr, D), shape(per, Sr, D),
         ],
-        in_specs=[inside] * 3 + [anywhere] * 2,
+        in_specs=[inside] * 5,
         out_specs=[anywhere] * 7,
-        scratch_shapes=[
-            pltpu.VMEM((per, Hr, D), BF16), pltpu.VMEM((per, Sr, D), BF16), dma((9,))
-        ],
-        compiler_params=pltpu.CompilerParams(vmem_limit_bytes=1 << 25),
+        scratch_shapes=[dma((7,))],
+        compiler_params=pltpu.CompilerParams(vmem_limit_bytes=1 << 22),
     )(
-        *[pltpu.with_memory_space_constraint(o, vmem) for o in outs[:3]],
-        *[pltpu.with_memory_space_constraint(o, pltpu.MemorySpace.HBM) for o in outs[3:]],
+        *[pltpu.with_memory_space_constraint(o, vmem) for o in outs],
     )
     return (
         eg.reshape(1, D, Hc), eu.reshape(1, D, Hc), ed.reshape(1, per * Hr, D),

time: 291 us -> 289 us (level)
  no operation moved by 1% of the time
where the time goes in v4:
time: 289 us; the launch traced here: 288 us
  Pallas kernels  288 us (100%)
    pallas_call x1, Pallas kernels, on_device(): pl.pallas_call(functools.partial(kernel, S), out_shape=[vmem(dims, BF16)...  283 us

profile of v4, /device:TPU:20, one launch (start us, length us, event | category | flops | bytes accessed | tf_op | source)
XLA Modules:
  0.0 288.4 jit_solution(15102822363033173196)
XLA Ops:
  0.6 282.6 %shard_map.153 = (bf16[8,512,512]{2,1,0:T(8,128)(2,1)S(1)}, bf16[8,512,512]{2,1,0:T(8,128)(2,1)S(1)}, bf16[512,1024]{1,0:T(8,128)(2,1)S(1)}, bf16[2,128,4096]{2,1,0:T(8,128)(2,1)S(1)}, bf16[2,128,4096]{2,1,0:T(8,128)(2,1)S(1)}) custom-call(bf16[512,4096]{1,0:T(8,128)(2,1)} %tokens.1, f32[8,512,256]{2,1,0:T(8,128)} %gate_t.1, f32[8,512,256]{2,1,0:T(8,128)} %up_t.1, ...), custom_call_target="tpu_custom_call" | custom-call | flops 15032385536 | bytes 67108864 | tf_op jit(solution)/shard_map/pallas_call | solution.py:724
  283.3 5.0 %shard_map.154 = (bf16[8,512,256]{2,1,0:T(8,128)(2,1)}, bf16[8,512,256]{2,1,0:T(8,128)(2,1)}, bf16[8,512,256]{2,1,0:T(8,128)(2,1)}, bf16[8,512,256]{2,1,0:T(8,12...) custom-call(bf16[8,512,512]{2,1,0:T(8,128)(2,1)S(1)} %get-tuple-element.19.gub, ...), custom_call_target="tpu_custom_call" | custom-call | tf_op jit(solution)/shard_map/pallas_call | solution.py:738

commit v5 on v4

--- a/solution.py
+++ b/solution.py
@@ -391,6 +391,11 @@
         shared_hop(Z - 1)
     loop(half, lambda k: sent(gst.at[k], gu_s.at[k]), half // 2)
 
+    @pl.when(inner)
+    def _():
+        loop(half, send_dn)
+
+
     def act(v, width):
         gate, up = v[:, :width], v[:, width:]
         return (gate / (1.0 + jnp.exp(-gate)) * up).astype(BF16)
@@ -422,7 +427,11 @@
         arrived(gub.at[s], gu_r.at[s])
 
     loop(E - 1, wait_gu)
-    loop(half, send_dn)
+
+    @pl.when(jnp.logical_not(inner))
+    def _():
+        loop(half, send_dn)
+
     M, g, groups = S.M, S.g, S.groups
     own = f // g
 
@@ -545,11 +554,11 @@
     def _():
         to = over_z * Y + y
         cmb[f % half] = res_at(to)[...]
+        many = half * cap
+        shares = weigh(over_z, f // half * many, many)
         for i in range(1, half):
             e = (f + i) % half
             arrived(cmb.at[e], cmb_r.at[e])
-        many = half * cap
-        shares = weigh(over_z, f // half * many, many)
 
         def part(n):
             at = pl.ds(pl.multiple_of(n * nt, nt), nt)

time: 289 us -> 289 us (level)
  no operation moved by 1% of the time
where the time goes in v5:
time: 289 us; the launch traced here: 287 us
  Pallas kernels  286 us (99%)
    pallas_call x1, Pallas kernels, on_device(): pl.pallas_call(functools.partial(kernel, S), out_shape=[vmem(dims, BF16)...  281 us

profile of v5, /device:TPU:20, one launch (start us, length us, event | category | flops | bytes accessed | tf_op | source)
XLA Modules:
  0.0 287.2 jit_solution(4469745091561382167)
XLA Ops:
  0.6 281.4 %shard_map.153 = (bf16[8,512,512]{2,1,0:T(8,128)(2,1)S(1)}, bf16[8,512,512]{2,1,0:T(8,128)(2,1)S(1)}, bf16[512,1024]{1,0:T(8,128)(2,1)S(1)}, bf16[2,128,4096]{2,1,0:T(8,128)(2,1)S(1)}, bf16[2,128,4096]{2,1,0:T(8,128)(2,1)S(1)}) custom-call(bf16[512,4096]{1,0:T(8,128)(2,1)} %tokens.1, f32[8,512,256]{2,1,0:T(8,128)} %gate_t.1, f32[8,512,256]{2,1,0:T(8,128)} %up_t.1, ...), custom_call_target="tpu_custom_call" | custom-call | flops 15032385536 | bytes 67108864 | tf_op jit(solution)/shard_map/pallas_call | solution.py:733
  282.1 5.0 %shard_map.154 = (bf16[8,512,256]{2,1,0:T(8,128)(2,1)}, bf16[8,512,256]{2,1,0:T(8,128)(2,1)}, bf16[8,512,256]{2,1,0:T(8,128)(2,1)}, bf16[8,512,256]{2,1,0:T(8,12...) custom-call(bf16[8,512,512]{2,1,0:T(8,128)(2,1)S(1)} %get-tuple-element.19.gub, ...), custom_call_target="tpu_custom_call" | custom-call | tf_op jit(solution)/shard_map/pallas_call | solution.py:747
